TPU v7x, 128 devices: a whole 4x4x4 slice. The times are simulated.
128 devices in a mesh: kv: 16 (over z, x), tp: 8 (over y, core).
Axes of the slice: x: 4, y: 4, z: 4, core: 2. Of those that a mesh axis runs over, the one named last changes fastest.
Arguments:
- tokens: bfloat16 [64, 2048], P(None, 'kv'), may hold values from -6 to 6
- token_gain: float32 [2048], P('kv'), may hold values from 0.1 to 1.9
- w_query: bfloat16 [2048, 1536], P('kv', 'tp'), may hold values from -0.125 to 0.125
- w_down_kv: bfloat16 [2048, 512], P('kv'), may hold values from -0.125 to 0.125
- w_rope_key: bfloat16 [2048, 64], P('kv'), may hold values from -0.125 to 0.125
- latent_gain: float32 [512], replicated, may hold values from 0.1 to 1.9
- w_key_up: bfloat16 [8, 512, 128], P('tp'), may hold values from -0.25 to 0.25
- w_value_up: bfloat16 [8, 512, 128], P('tp'), may hold values from -0.25 to 0.25
- w_out: bfloat16 [1024, 2048], P('tp', 'kv'), may hold values from -0.1875 to 0.1875
- out_gain: float32 [2048], P('kv'), may hold values from 0.1 to 1.9
- cache_latent: bfloat16 [64, 8192, 512], P('tp', 'kv'), may hold values from -6 to 6
- cache_rope: bfloat16 [64, 8192, 64], P('tp', 'kv'), may hold values from -6 to 6
- lengths: int32 [64], replicated, may hold values from 1 to 8191, as said below
Outputs:
- mixed: bfloat16 [64, 2048], P(None, 'kv')
Inputs may be any that keep to these rules, and one draw needn't show every extreme that they name: `lengths`: each of the 64 sequences has 1 to 8191 cached positions; some sequence has exactly 8191 and some exactly 1.
All inputs are finite; a program needn't handle non-finite values.
Results may differ from a plain program's by a relative error of at most 0.015.
Values may be sent and summed in bfloat16 or wider, within the bound.
A program may use at most 64 MiB of HBM per device.

v0:
```python
import functools

import jax
import jax.numpy as jnp
from jax import lax
from jax.sharding import Mesh
from jax.sharding import PartitionSpec as P

KV = ("kv_0", "kv_1")


EPSILON = 1e-06
NEGATIVE = -1e30


def over_pieces(value, axis):
    parts = lax.all_gather(value, axis)
    return parts.sum(axis=0)


def by_axis(value, axes):
    return functools.reduce(lax.pmax, axes, value)


def over_axes(value, axes):
    for axis in axes:
        value = lax.psum(value, axis)
    return value


def rotate_half(values, cosine, sine_table):
    half_width = values.shape[-1] // 2
    lower_half = values[..., :half_width]
    upper_half = values[..., half_width:]
    return jnp.concatenate(
        [
            lower_half * cosine - upper_half * sine_table,
            upper_half * cosine + lower_half * sine_table,
        ],
        axis=-1,
    )


def angle_tables(lengths, rope_width):
    inverse_freq = 1.0 / 10000.0 ** (jnp.arange(0, rope_width, 2, dtype=jnp.float32) / rope_width)
    angles = lengths.astype(jnp.float32)[:, None] * inverse_freq[None, :]
    return (jnp.cos(angles), jnp.sin(angles))


def on_device(
    tokens,
    token_gain,
    w_query,
    w_down_kv,
    w_rope_key,
    latent_gain,
    w_key_up,
    w_value_up,
    w_out,
    out_gain,
    cache_latent,
    cache_rope,
    lengths,
):
    model_width = tokens.shape[1] * lax.axis_size(KV)
    seq_count = tokens.shape[0]
    local_heads, latent_width, nope_width = w_key_up.shape
    rope_width = w_rope_key.shape[1]
    head_width = nope_width + rope_width
    factor = head_width ** (-0.5)
    token_values = tokens.astype(jnp.float32)
    scaled = (token_values * token_gain).astype(jnp.bfloat16)
    query_part = jnp.dot(scaled, w_query, preferred_element_type=jnp.float32)
    latent_part = jnp.dot(scaled, w_down_kv, preferred_element_type=jnp.float32)
    rope_part = jnp.dot(scaled, w_rope_key, preferred_element_type=jnp.float32)
    query_raw, latent_raw, rope_raw = (
        over_pieces(query_part, KV),
        over_pieces(latent_part, KV),
        over_pieces(rope_part, KV),
    )
    query_heads = query_raw.astype(jnp.bfloat16).reshape(seq_count, local_heads, head_width)
    latent = (
        latent_raw
        * lax.rsqrt(jnp.mean(latent_raw * latent_raw, axis=1, keepdims=True) + EPSILON)
        * latent_gain
    ).astype(jnp.bfloat16)
    cosine, sine_table = angle_tables(lengths, rope_width)
    new_rope = rotate_half(rope_raw, cosine, sine_table).astype(jnp.bfloat16)
    query_nope = query_heads[..., :nope_width]
    query_rope = rotate_half(
        query_heads[..., nope_width:].astype(jnp.float32),
        cosine[:, None, :],
        sine_table[:, None, :],
    ).astype(jnp.bfloat16)
    query_latent = jnp.einsum(
        "bhn,hcn->bhc", query_nope, w_key_up, preferred_element_type=jnp.float32
    ).astype(jnp.bfloat16)
    seq_latent, seq_rope = (
        lax.all_to_all(query_latent, "tp", split_axis=0, concat_axis=1, tiled=True),
        lax.all_to_all(query_rope, "tp", split_axis=0, concat_axis=1, tiled=True),
    )
    local_seqs = cache_latent.shape[0]
    local_pos = cache_latent.shape[1]
    first_row = lax.axis_index("tp") * local_seqs
    own_latent = lax.dynamic_slice_in_dim(latent, first_row, local_seqs, 0)
    own_rope = lax.dynamic_slice_in_dim(new_rope, first_row, local_seqs, 0)
    own_length = lax.dynamic_slice_in_dim(lengths, first_row, local_seqs, 0)
    first_pos = lax.axis_index(KV) * local_pos
    positions = first_pos + jnp.arange(local_pos, dtype=jnp.int32)
    scores = (
        jnp.einsum("bhc,blc->bhl", seq_latent, cache_latent, preferred_element_type=jnp.float32)
        + jnp.einsum("bhr,blr->bhl", seq_rope, cache_rope, preferred_element_type=jnp.float32)
    ) * factor
    visible = positions[None, None, :] < own_length[:, None, None]
    new_score = (
        jnp.einsum("bhc,bc->bh", seq_latent, own_latent, preferred_element_type=jnp.float32)
        + jnp.einsum("bhr,br->bh", seq_rope, own_rope, preferred_element_type=jnp.float32)
    ) * factor
    holder = ((own_length >= first_pos) & (own_length < first_pos + local_pos))[:, None]
    local_max = jnp.maximum(
        jnp.max(jnp.where(visible, scores, NEGATIVE), axis=2),
        jnp.where(holder, new_score, NEGATIVE),
    )
    weights = jnp.where(visible, jnp.exp(scores - local_max[..., None]), 0.0)
    new_weight = jnp.where(holder, jnp.exp(new_score - local_max), 0.0)
    weight_sum = jnp.sum(weights, axis=2) + new_weight
    rounded_new = lax.optimization_barrier(new_weight.astype(jnp.bfloat16)).astype(jnp.float32)
    weighted = (
        jnp.einsum(
            "bhl,blc->bhc",
            weights.astype(jnp.bfloat16),
            cache_latent,
            preferred_element_type=jnp.float32,
        )
        + rounded_new[..., None] * own_latent.astype(jnp.float32)[:, None, :]
    )
    global_max = by_axis(local_max, KV)
    rescale = jnp.exp(local_max - global_max)
    weight_sum, weighted = (
        over_pieces(weight_sum * rescale, KV),
        over_pieces(weighted * rescale[..., None], KV),
    )
    head_latent = (weighted / weight_sum[..., None]).astype(jnp.bfloat16)
    batch_latent = lax.all_to_all(head_latent, "tp", split_axis=1, concat_axis=0, tiled=True)
    head_out = (
        jnp.einsum("bhc,hcv->bhv", batch_latent, w_value_up, preferred_element_type=jnp.float32)
        .astype(jnp.bfloat16)
        .reshape(seq_count, -1)
    )
    mixed_sum = over_pieces(jnp.dot(head_out, w_out, preferred_element_type=jnp.float32), "tp")
    out_squares = over_axes(jnp.sum(mixed_sum * mixed_sum, axis=1), KV)
    return (mixed_sum * lax.rsqrt(out_squares / model_width + EPSILON)[:, None] * out_gain).astype(
        jnp.bfloat16
    )


def solution(mesh):
    finer = Mesh(mesh.devices.reshape(4, 4, mesh.shape["tp"]), ("kv_0", "kv_1", "tp"))
    return jax.shard_map(
        on_device,
        mesh=finer,
        in_specs=(
            P(None, KV),
            P(KV),
            P(KV, "tp"),
            P(KV, None),
            P(KV, None),
            P(),
            P("tp", None, None),
            P("tp", None, None),
            P("tp", KV),
            P(KV),
            P("tp", KV, None),
            P("tp", KV, None),
            P(),
        ),
        out_specs=P(None, KV),
        check_vma=False,
    )
```

profile of v0, /device:TPU:1, one launch (start us, length us, event | category | flops | bytes accessed | tf_op | source)
XLA Modules:
  0.0 198.3 jit_solution(11221222304284880200)
XLA Ops:
  6.5 1.8 fusion.47
  8.4 0.7 convert_element_type.83
  9.0 1.0 fusion.48
  10.0 23.8 %all-gather = f32[1024,192]{1,0:T(8,128)S(1)} all-gather(f32[64,192]{1,0:T(8,128)S(1)} %fusion.48), channel_id=2, replica_groups=mesh['kv_0'=4,'kv_1'=4,'tp'=8] {'kv_0','kv_1'}, dimensions={0}, use_global_device_ids=true | all-gather | bytes 835584 | tf_op jit(solution)/shard_map/all_gather | solution.py:17
  34.0 0.2 fusion.34
  34.1 0.6 broadcast.112
  34.7 0.7 reduce.1
  35.5 0.7 reshape.207
  36.2 9.5 %all-to-all-start.1 = ((bf16[8,2,256]{2,1,0:T(2,128)(2,1)}), bf16[8,2,256]{2,1,0:T(2,128)(2,1)S(1)}, u32[]{:S(2)}, u32[]{:S(2)}) async-start(bf16[8,2,256]{2,1,0:T(2,128)(2,1)} %reshape.207), calls=%async_computation.1 | async-start | bytes 16384 | tf_op jit(solution)/shard_map/all_to_all | solution.py:100
  45.7 0.9 fusion.46
  46.6 19.4 %all-gather.2 = f32[1024,64]{1,0:T(8,128)S(1)} all-gather(f32[64,64]{1,0:T(8,128)S(1)} %fusion.46), channel_id=4, replica_groups=mesh['kv_0'=4,'kv_1'=4,'tp'=8] {'kv_0','kv_1'}, dimensions={0}, use_global_device_ids=true | all-gather | bytes 278528 | tf_op jit(solution)/shard_map/all_gather | solution.py:17
  66.3 0.2 fusion.2
  66.9 0.7 reduce
  67.6 0.6 reshape.205
  68.3 8.7 %all-to-all-start = ((bf16[8,2,2048]{2,1,0:T(2,128)(2,1)}), bf16[8,2,2048]{2,1,0:T(2,128)(2,1)S(1)}, u32[]{:S(2)}, u32[]{:S(2)}) async-start(bf16[8,2,2048]{2,1,0:T(2,128)(2,1)} %reshape.205), calls=%async_computation | async-start | bytes 131072 | tf_op jit(solution)/shard_map/all_to_all | solution.py:99
  77.3 4.6 %all-to-all-done = bf16[8,2,2048]{2,1,0:T(2,128)(2,1)S(1)} async-done(((bf16[8,2,2048]{2,1,0:T(2,128)(2,1)}), bf16[8,2,2048]{2,1,0:T(2,128)(2,1)S(1)}, u32[]{:S(2)}, u32[]{:S(2)}) %all-to-all-start) | async-done | bytes 65568 | tf_op jit(solution)/shard_map/all_to_all | solution.py:99
  82.0 3.4 %fusion.14 = f32[8,8,512]{2,1,0:T(8,128)S(1)} fusion(bf16[8,512,512]{2,1,0:T(8,128)(2,1)} %param.23, bf16[8,8,1,512]{3,1,0,2:T(8,128)(2,1)S(1)} %bitcast.77), kind=kOutput, calls=%fused_computation.21 | convolution fusion | flops 33554432 | bytes 4390912 | tf_op jit(solution)/shard_map/bhc,blc->bhl/dot_general | solution.py:111
  85.3 0.3 select_reduce_fusion
  85.6 1.8 reduce_sum.82
  87.9 6.8 %pmax.14 = f32[8,8]{1,0:T(8,128)S(1)} all-reduce(f32[8,8]{1,0:T(8,128)S(1)} %select_maximum_fusion), channel_id=1, replica_groups=mesh['kv_0'=4,'kv_1'=4,'tp'=8] {'kv_0'}, use_global_device_ids=true, to_apply=%region_5.6 | all-reduce | flops 64 | bytes 512 | tf_op jit(solution)/shard_map/pmax | solution.py:22
  94.7 0.2 fusion.7
  94.9 7.8 %pmax.15 = f32[8,8]{1,0:T(8,128)S(1)} all-reduce(f32[8,8]{1,0:T(8,128)S(1)} %pmax.14), channel_id=1, replica_groups=mesh['kv_0'=4,'kv_1'=4,'tp'=8] {'kv_1'}, use_global_device_ids=true, to_apply=%region_6.7 | all-reduce | flops 64 | bytes 512 | tf_op jit(solution)/shard_map/pmax | solution.py:22
  102.8 3.5 %fusion.1 = f32[8,8,512]{2,1,0:T(8,128)} fusion(bf16[8,512,512]{2,1,0:T(8,128)(2,1)} %param.23, f32[8,8,512]{2,1,0:T(8,128)S(1)} %get-tuple-element.19, f32[8,8]{1,0:T(8,128)S(1)} %get-tuple-element.7, f32[8,512]{1,0:T(8,128)S(1)} %get-tuple-element.10, f32[8,8]{1,0:T(8,128)S(1)} %convert_element_type.87, f32[8,8]{1,0:T(8,128)S(1)} %select_maximum_fusion, ...), kind=kOutput, calls=%fused_computation.3 | convolution fusion | flops 33751040 | bytes 4477696 | tf_op jit(solution)/shard_map/bhl,blc->bhc/dot_general | solution.py:129
  106.4 15.6 %all-gather.4 = f32[128,8]{1,0:T(8,128)S(1)} all-gather(f32[8,8]{1,0:T(8,128)S(1)} %get-tuple-element.5), channel_id=6, replica_groups=mesh['kv_0'=4,'kv_1'=4,'tp'=8] {'kv_0','kv_1'}, dimensions={0}, use_global_device_ids=true | all-gather | bytes 4352 | tf_op jit(solution)/shard_map/all_gather | solution.py:17
  122.0 26.9 %all-gather.11.cloned.1.call-done = f32[128,8,512]{2,1,0:T(8,128)} async-done(((f32[8,8,512]{2,1,0:T(8,128)}), f32[128,8,512]{2,1,0:T(8,128)}) %all-gather.11.cloned.1.call-update) | async-done | bytes 2097168 | tf_op jit(solution)/shard_map/all_gather | solution.py:17
  149.0 1.8 reduce_sum.85
  150.8 11.4 %all_to_all.51 = bf16[8,8,512]{2,0,1:T(8,128)(2,1)S(1)} all-to-all(bf16[8,8,512]{2,0,1:T(8,128)(2,1)S(1)} %copy.43), channel_id=1, replica_groups=mesh['kv_0'=4,'kv_1'=4,'tp'=8] {'tp'}, dimensions={1} | all-to-all | bytes 131072 | tf_op jit(solution)/shard_map/all_to_all | solution.py:144
  162.3 0.3 fusion.3
  162.5 13.4 %all-gather.5 = f32[512,128]{1,0:T(8,128)S(1)} all-gather(f32[64,128]{1,0:T(8,128)S(1)} %fusion.3), channel_id=7, replica_groups=mesh['kv_0'=4,'kv_1'=4,'tp'=8] {'tp'}, dimensions={0}, use_global_device_ids=true | all-gather | bytes 294912 | tf_op jit(solution)/shard_map/all_gather | solution.py:17
  176.1 8.1 %psum.14 = f32[64]{0:T(128)S(1)} all-reduce(f32[64]{0:T(128)S(1)} %multiply_reduce_fusion.1), channel_id=1, replica_groups=mesh['kv_0'=4,'kv_1'=4,'tp'=8] {'kv_0'}, use_global_device_ids=true, to_apply=%region_12.13 | all-reduce | flops 64 | bytes 512 | tf_op jit(solution)/shard_map/psum | solution.py:27
  184.2 6.5 %psum.15 = f32[64]{0:T(128)S(1)} all-reduce(f32[64]{0:T(128)S(1)} %psum.14), channel_id=1, replica_groups=mesh['kv_0'=4,'kv_1'=4,'tp'=8] {'kv_1'}, use_global_device_ids=true, to_apply=%region_13.14 | all-reduce | flops 64 | bytes 512 | tf_op jit(solution)/shard_map/psum | solution.py:27
  190.8 0.7 multiply_convert_fusion
  (56 shorter events, 2.2 us)
Async XLA Ops:
  6.5 78.8 %copy-start = (bf16[8,512,64]{1,2,0:T(8,128)(2,1)S(1)}, bf16[8,512,64]{1,2,0:T(8,128)(2,1)}, u32[]{:S(2)}) copy-start(bf16[8,512,64]{1,2,0:T(8,128)(2,1)} %param.24) | copy-start | bytes 1572868
  6.5 59.7 %copy-start.6 = (s32[64]{0:T(128)S(1)}, s32[64]{0:T(128)}, u32[]{:S(2)}) copy-start(s32[64]{0:T(128)} %param.25) | copy-start | bytes 772
  6.5 59.8 %copy-start.2 = (bf16[1,512,128]{2,1,0:T(8,128)(2,1)S(1)}, bf16[1,512,128]{2,1,0:T(8,128)(2,1)}, u32[]{:S(2)}) copy-start(bf16[1,512,128]{2,1,0:T(8,128)(2,1)} %param.19) | copy-start | bytes 393220
  6.5 79.1 %all-gather.9.cloned.1.call-start = ((), (), s32[]{:S(2)}) async-start(), calls=%async_computation.3 | async-start | bytes 2228224 | tf_op jit(solution)/shard_map/all_gather | solution.py:17
  36.2 32.1 %all-to-all-start.1 = ((bf16[8,2,256]{2,1,0:T(2,128)(2,1)}), bf16[8,2,256]{2,1,0:T(2,128)(2,1)S(1)}, u32[]{:S(2)}, u32[]{:S(2)}) async-start(bf16[8,2,256]{2,1,0:T(2,128)(2,1)} %reshape.207), calls=%async_computation.1 | async-start | bytes 16384 | tf_op jit(solution)/shard_map/all_to_all | solution.py:100
  67.6 20.0 %copy-start.4 = (f32[512]{0:T(512)S(1)}, f32[512]{0:T(512)}, u32[]{:S(2)}) copy-start(f32[512]{0:T(512)} %param.18) | copy-start | bytes 6148
  68.3 13.6 %all-to-all-start = ((bf16[8,2,2048]{2,1,0:T(2,128)(2,1)}), bf16[8,2,2048]{2,1,0:T(2,128)(2,1)S(1)}, u32[]{:S(2)}, u32[]{:S(2)}) async-start(bf16[8,2,2048]{2,1,0:T(2,128)(2,1)} %reshape.205), calls=%async_computation | async-start | bytes 131072 | tf_op jit(solution)/shard_map/all_to_all | solution.py:99
  77.0 71.9 %all-gather.11.cloned.1.call-start = ((), (), s32[]{:S(2)}) async-start(), calls=%async_computation.4 | async-start | bytes 2228224 | tf_op jit(solution)/shard_map/all_gather | solution.py:17
  87.4 74.9 %copy-start.1 = (bf16[1,512,128]{2,1,0:T(8,128)(2,1)S(1)}, bf16[1,512,128]{2,1,0:T(8,128)(2,1)}, u32[]{:S(2)}) copy-start(bf16[1,512,128]{2,1,0:T(8,128)(2,1)} %param.20) | copy-start | bytes 393220
  87.4 74.9 %copy-start.3 = (bf16[128,128]{1,0:T(8,128)(2,1)S(1)}, bf16[128,128]{1,0:T(8,128)(2,1)}, u32[]{:S(2)}) copy-start(bf16[128,128]{1,0:T(8,128)(2,1)} %param.21) | copy-start | bytes 98308
  102.7 88.0 %copy-start.5 = (f32[128]{0:T(128)S(1)}, f32[128]{0:T(128)}, u32[]{:S(2)}) copy-start(f32[128]{0:T(128)} %param.22) | copy-start | bytes 1540
Sparse Core Ops, SparseCore 0:
  9.5 46.8 all-gather.8
  106.5 42.4 all-gather.10
where the time goes:
time: 202 us; the launch traced here: 198 us
  blocking collectives  113 us (56%)
  waiting for transfers between devices  31.6 us (16%)
  starting transfers between devices  18.3 us (9%)
  between operations  13.6 us (7%)
  matrix products  11.6 us (6%)
  other arithmetic  7.71 us (4%)
  local copies, waits for them, and re-layouts  2.71 us (1%)
    all_gather x4, blocking collectives, over_pieces(): parts = lax.all_gather(value, axis)  72.2 us
    all_gather x2, waiting for transfers between devices, over_pieces(): parts = lax.all_gather(value, axis)  26.9 us
    pmax x2, blocking collectives, by_axis(): return functools.reduce(lax.pmax, axes, value)  14.7 us
    psum x2, blocking collectives, over_axes(): value = lax.psum(value, axis)  14.6 us
    all_to_all x1, blocking collectives, on_device(): lax.all_to_all(head_latent, 'tp', split_axis=1, concat_axis=0, tiled=True)  11.4 us
    all_to_all x1, starting transfers between devices, on_device(): lax.all_to_all(query_rope, 'tp', split_axis=0, concat_axis=1, tiled=True)  9.5 us
    all_to_all x1, starting transfers between devices, on_device(): lax.all_to_all(query_latent, 'tp', split_axis=0, concat_axis=1, tiled=True)  8.74 us
    all_to_all x1, waiting for transfers between devices, on_device(): lax.all_to_all(query_latent, 'tp', split_axis=0, concat_axis=1, tiled=True)  4.63 us
  transfers between devices with their start and end apart: 4, of which 2 were waited for; matrix products, arithmetic and copies ran while one was open for 6% of the time, Pallas kernels for 0%

commit v1 on v0

v1 whole, which is shorter than its diff:
```python
import functools

import jax
import jax.numpy as jnp
import numpy as np
from jax import lax
from jax.experimental import pallas as pl
from jax.experimental.pallas import tpu as pltpu
from jax.sharding import PartitionSpec as P

MESH = pl.DeviceIdType.MESH
EPSILON = 1e-06
NEGATIVE = -1e30
BF16 = jnp.bfloat16
F32 = jnp.float32


def dot(a, b):
    return jnp.dot(a, b, preferred_element_type=F32)


def dot_nt(a, b):
    return lax.dot_general(a, b, (((1,), (1,)), ((), ())), preferred_element_type=F32)


def iota(shape, axis):
    return lax.broadcasted_iota(jnp.int32, shape, axis)


def to_column(row, rows):
    picked = iota((rows, rows), 0) == iota((rows, rows), 1)
    return jnp.sum(jnp.where(picked, row[:, :rows], 0.0), axis=1, keepdims=True)


def to_row(column, rows):
    picked = iota((rows, 128), 0) == iota((rows, 128), 1)
    return jnp.sum(jnp.where(picked, column, 0.0), axis=0, keepdims=True)


def kernel(
    tok_h, tgain_h, wq_h, wd_h, wr_h, lgain_h, wk_h, wv_h, wo_h, ogain_h, cl_h, cr_h, len_h, freq_h,
    out_ref,
    tok, tgain, wq, wd, wr, lgain, wk, wv, wo, ogain, cl, cr, lens, freq,
    len_tab, cos_tab, sin_tab,
    a1_send, a1_recv, a2_send, a2_recv,
    lat_all, lat_send, lat_recv,
    b_send, b_recv, q_tab, o_tab, d_send, d_recv,
    c1_send, c1_recv, c1_lse, c1_lser, c2_send, c2_recv, c2_lse, c2_lser,
    f_recv, f_send, g_send, g_recv,
    load_sem, cache_sem,
    a1_ss, a1_rs, a2_ss, a2_rs, lat_ss, lat_rs, b_ss, b_rs, d_ss, d_rs,
    c1_ss, c1_rs, c2_ss, c2_rs, cl1_ss, cl1_rs, cl2_ss, cl2_rs, f_ss, f_rs, g_ss, g_rs,
):
    kv = lax.axis_index("kv")
    tp = lax.axis_index("tp")
    z = kv // 4
    x = kv % 4

    barrier = pltpu.get_barrier_semaphore()

    def greet_kv(d, c):
        pl.semaphore_signal(barrier, inc=1, device_id=((kv + d) % 16, tp), device_id_type=MESH)
        return c

    def greet_tp(d, c):
        pl.semaphore_signal(barrier, inc=1, device_id=(kv, (tp + d) % 8), device_id_type=MESH)
        return c

    lax.fori_loop(1, 16, greet_kv, 0)
    lax.fori_loop(1, 8, greet_tp, 0)

    pairs = [
        (tok_h, tok), (tgain_h, tgain), (wq_h, wq), (len_h, lens), (freq_h, freq), (wd_h, wd), (wr_h, wr),
        (wk_h, wk), (lgain_h, lgain), (wv_h, wv), (wo_h, wo), (ogain_h, ogain),
    ]
    loads = [pltpu.make_async_copy(s, d, load_sem.at[i]) for i, (s, d) in enumerate(pairs)]
    for copy in loads:
        copy.start()
    cache_loads = []
    for s in range(8):
        cache_loads.append(pltpu.make_async_copy(cl_h.at[s], cl.at[s], cache_sem.at[s]))
        cache_loads.append(pltpu.make_async_copy(cr_h.at[s], cr.at[s], cache_sem.at[8 + s]))
    for copy in cache_loads:
        copy.start()

    for i in range(3):
        loads[i].wait()
    scaled = (tok[...].astype(F32) * tgain[...]).astype(BF16)
    q_part = dot(scaled, wq[...])
    rope_part = q_part[:, 128:192]
    q_nope_part = q_part[:, :128]
    q_rope_part = jnp.concatenate([rope_part[:32], rope_part[32:]], axis=1)
    a1_send[0:64, :] = q_nope_part.astype(BF16)
    a1_send[64:96, :] = q_rope_part.astype(BF16)

    pl.semaphore_wait(barrier, 22)

    def x_dev(d):
        return (z * 4 + (x + d) % 4, tp)

    def z_dev(d):
        return (((z + d) % 4) * 4 + x, tp)

    def line(src, dst, ss, rs, dev):
        return [
            pltpu.make_async_remote_copy(
                src_ref=src, dst_ref=dst.at[d - 1], send_sem=ss.at[d - 1], recv_sem=rs.at[d - 1],
                device_id=dev(d), device_id_type=MESH,
            )
            for d in (1, 2, 3)
        ]

    a1 = line(a1_send, a1_recv, a1_ss, a1_rs, x_dev)
    for copy in a1:
        copy.start()

    for i in range(3, 7):
        loads[i].wait()
    lat_all[:, 0:512] = dot(scaled, wd[...])
    lat_all[:, 512:576] = dot(scaled, wr[...])
    lat_all[:, 576:640] = jnp.zeros((64, 64), F32)
    mine = lat_all[pl.ds(pl.multiple_of(tp * 8, 8), 8), :]
    for r in range(8):
        lat_send[r] = mine[r : r + 1, :]
    lat_recv[kv] = lat_send[kv // 2]

    def lat_copy(d):
        to = (kv + d) % 16
        return pltpu.make_async_remote_copy(
            src_ref=lat_send.at[to // 2], dst_ref=lat_recv.at[kv], send_sem=lat_ss.at[d], recv_sem=lat_rs.at[kv],
            device_id=(to, tp), device_id_type=MESH,
        )

    def lat_start(d, c):
        lat_copy(d).start()
        return c

    lax.fori_loop(1, 16, lat_start, 0)

    len_col = to_column(lens[...].astype(F32), 64)
    len_tab[...] = jnp.broadcast_to(len_col, (64, 128))
    lane = iota((32, 128), 1)
    packed_len = jnp.where(lane < 64, len_col[:32], len_col[32:])
    angle = packed_len * freq[...]
    cosine = jnp.cos(angle)
    sine = jnp.sin(angle)
    sine = jnp.where(lane % 64 < 32, -sine, sine)
    cos_tab[0:32, :] = cosine[:, :64]
    cos_tab[32:64, :] = cosine[:, 64:]
    sin_tab[0:32, :] = sine[:, :64]
    sin_tab[32:64, :] = sine[:, 64:]

    def added(own, recv, rows):
        total = own
        for d in range(3):
            total = total + recv[d, rows, :].astype(F32)
        return total

    for copy in a1:
        copy.wait_recv()
    q_nope_sum = added(q_nope_part, a1_recv, slice(0, 64))
    q_rope_sum = added(q_rope_part, a1_recv, slice(64, 96))
    a2_send[0:64, :] = q_nope_sum.astype(BF16)
    a2_send[64:96, :] = q_rope_sum.astype(BF16)
    a2 = line(a2_send, a2_recv, a2_ss, a2_rs, z_dev)
    for copy in a2:
        copy.start()
    for copy in a2:
        copy.wait_recv()
    q_nope = added(q_nope_sum, a2_recv, slice(0, 64)).astype(BF16)
    q_rope = added(q_rope_sum, a2_recv, slice(64, 96)).astype(BF16).astype(F32)
    swapped = jnp.where(lane % 64 < 32, pltpu.roll(q_rope, 96, 1), pltpu.roll(q_rope, 32, 1))
    q_rope = q_rope * cosine + swapped * sine
    q_rope = jnp.concatenate([q_rope[:, :64], q_rope[:, 64:]], axis=0)

    loads[7].wait()
    q_lat = dot_nt(q_nope, wk[...])
    pad = jnp.zeros((8, 64), F32)
    for j in range(8):
        block = jnp.concatenate([q_lat[8 * j : 8 * j + 8], q_rope[8 * j : 8 * j + 8], pad], axis=1)
        b_send[j] = block.astype(BF16)

    def tp_copy(d, src, dst, ss, rs):
        to = (tp + d) % 8
        return pltpu.make_async_remote_copy(
            src_ref=src.at[to], dst_ref=dst.at[tp], send_sem=ss.at[d], recv_sem=rs.at[tp],
            device_id=(kv, to), device_id_type=MESH,
        )

    def tp_wait_copy(d, src, dst, ss, rs):
        frm = (tp + d) % 8
        return pltpu.make_async_remote_copy(
            src_ref=src.at[frm], dst_ref=dst.at[frm], send_sem=ss.at[d], recv_sem=rs.at[frm],
            device_id=(kv, frm), device_id_type=MESH,
        )

    def tp_exchange(src, dst, ss, rs):
        for d in range(1, 8):
            tp_copy(d, src, dst, ss, rs).start()
        dst[tp] = src[tp]
        for d in range(1, 8):
            tp_wait_copy(d, src, dst, ss, rs).wait_recv()

    tp_exchange(b_send, b_recv, b_ss, b_rs)

    r64 = iota((64, 64), 0)
    c64 = iota((64, 64), 1)
    swap = (c64 == (r64 % 8) * 8 + r64 // 8).astype(BF16)
    queries = jnp.concatenate([b_recv[h].astype(F32) for h in range(8)], axis=0).astype(BF16)
    queries = dot(swap, queries)
    for s in range(8):
        q_tab[s] = queries[8 * s : 8 * s + 8]

    def lat_wait(d, c):
        frm = (kv + d) % 16
        pltpu.make_async_remote_copy(
            src_ref=lat_send.at[kv // 2], dst_ref=lat_recv.at[frm], send_sem=lat_ss.at[d], recv_sem=lat_rs.at[frm],
            device_id=(frm, tp), device_id_type=MESH,
        ).wait_recv()
        return c

    lax.fori_loop(1, 16, lat_wait, 0)
    lat_sum = lat_recv[0]
    for k in range(1, 16):
        lat_sum = lat_sum + lat_recv[k]
    loads[8].wait()
    lat_raw = lat_sum[:, :512]
    latent = (
        lat_raw * lax.rsqrt(jnp.mean(lat_raw * lat_raw, axis=1, keepdims=True) + EPSILON) * lgain[...]
    ).astype(BF16).astype(F32)
    key_raw = lat_sum[:, 512:576]
    new_seq = kv // 2
    new_row = tp * 8 + new_seq
    key_swapped = jnp.concatenate([key_raw[:, 32:], key_raw[:, :32]], axis=1)
    new_rope = key_raw * cos_tab[pl.ds(new_row, 1), :] + key_swapped * sin_tab[pl.ds(new_row, 1), :]
    new_rope = new_rope.astype(BF16).astype(F32)
    factor = 192.0 ** (-0.5)
    q_new = q_tab[new_seq]
    new_score = (
        jnp.sum(q_new[:, :512] * latent, axis=1, keepdims=True)
        + jnp.sum(q_new[:, 512:576] * new_rope, axis=1, keepdims=True)
    ) * factor

    positions = (kv * 512 + iota((8, 512), 1)).astype(F32)
    lane8 = iota((8, 128), 1)
    for s in range(8):
        cache_loads[2 * s].wait()
        cache_loads[2 * s + 1].wait()
        q = q_tab[s].astype(BF16)
        scores = (dot_nt(q[:, :512], cl[s]) + dot_nt(q[:, 512:576], cr[s])) * factor
        length = len_tab[pl.ds(tp * 8 + s, 1), 0:1]
        visible = positions < length
        is_new = jnp.logical_and(new_seq == s, kv % 2 == 0)
        own_new = jnp.where(is_new, new_score, NEGATIVE)
        top = jnp.maximum(jnp.max(jnp.where(visible, scores, NEGATIVE), axis=1, keepdims=True), own_new)
        weights = jnp.where(visible, jnp.exp(scores - top), 0.0)
        new_weight = jnp.where(is_new, jnp.exp(own_new - top), 0.0)
        total = jnp.sum(weights, axis=1, keepdims=True) + new_weight
        acc = dot(weights.astype(BF16), cl[s]) + new_weight.astype(BF16).astype(F32) * latent
        some = total > 0.0
        safe = jnp.where(some, total, 1.0)
        lse = jnp.where(some, top + jnp.log(safe), NEGATIVE)
        hi = lse.astype(BF16).astype(F32)
        mid = (lse - hi).astype(BF16).astype(F32)
        low = lse - hi - mid
        o_tab[8 * s : 8 * s + 8, 0:512] = acc / safe
        o_tab[8 * s : 8 * s + 8, 512:640] = jnp.where(
            lane8 == 0, hi, jnp.where(lane8 == 1, mid, jnp.where(lane8 == 2, low, 0.0))
        )

    by_head = dot(swap, o_tab[...].astype(BF16))
    for h in range(8):
        d_send[h] = by_head[8 * h : 8 * h + 8].astype(BF16)
    tp_exchange(d_send, d_recv, d_ss, d_rs)

    parts = jnp.concatenate([d_recv[j].astype(F32) for j in range(8)], axis=0)
    lse = jnp.sum(parts[:, 512:640], axis=1, keepdims=True)
    loads[9].wait()
    value = dot(parts[:, :512].astype(BF16), wv[...])

    def combine(value, lse, send, recv, lse_send, lse_recv, sems, dev):
        send[...] = value.astype(BF16)
        lse_send[...] = to_row(lse, 64)
        copies = line(send, recv, sems[0], sems[1], dev)
        lse_copies = line(lse_send, lse_recv, sems[2], sems[3], dev)
        for copy in lse_copies + copies:
            copy.start()
        for copy in lse_copies:
            copy.wait_recv()
        others = [to_column(lse_recv[d], 64) for d in range(3)]
        top = lse
        for other in others:
            top = jnp.maximum(top, other)
        own_scale = jnp.exp(lse - top)
        scales = [jnp.exp(other - top) for other in others]
        total = own_scale + scales[0] + scales[1] + scales[2]
        for copy in copies:
            copy.wait_recv()
        merged = value * (own_scale / total)
        for d in range(3):
            merged = merged + recv[d].astype(F32) * (scales[d] / total)
        return merged, top + jnp.log(total), copies + lse_copies

    value, lse, c1 = combine(
        value, lse, c1_send, c1_recv, c1_lse, c1_lser, (c1_ss, c1_rs, cl1_ss, cl1_rs), x_dev
    )
    value, lse, c2 = combine(
        value, lse, c2_send, c2_recv, c2_lse, c2_lser, (c2_ss, c2_rs, cl2_ss, cl2_rs), z_dev
    )
    head_out = value.astype(BF16)

    loads[10].wait()
    f_send[...] = dot(head_out, wo[...]).astype(BF16)

    def f_copy(d, slot, to):
        return pltpu.make_async_remote_copy(
            src_ref=f_send, dst_ref=f_recv.at[slot], send_sem=f_ss.at[d], recv_sem=f_rs.at[slot],
            device_id=(kv, to), device_id_type=MESH,
        )

    for d in range(1, 8):
        f_copy(d, tp, (tp + d) % 8).start()
    f_recv[tp] = f_send[...]
    for d in range(1, 8):
        frm = (tp + d) % 8
        f_copy(d, frm, frm).wait_recv()
    mixed = f_recv[0].astype(F32)
    for h in range(1, 8):
        mixed = mixed + f_recv[h].astype(F32)

    g_send[...] = to_row(jnp.sum(mixed * mixed, axis=1, keepdims=True), 64)

    def g_copy(d, slot, to):
        return pltpu.make_async_remote_copy(
            src_ref=g_send, dst_ref=g_recv.at[slot], send_sem=g_ss.at[d], recv_sem=g_rs.at[slot],
            device_id=(to, tp), device_id_type=MESH,
        )

    def g_start(d, c):
        g_copy(d, kv, (kv + d) % 16).start()
        return c

    def g_wait(d, c):
        frm = (kv + d) % 16
        g_copy(d, frm, frm).wait_recv()
        return c

    lax.fori_loop(1, 16, g_start, 0)
    g_recv[kv] = g_send[...]
    loads[11].wait()
    lax.fori_loop(1, 16, g_wait, 0)
    squares = g_recv[0]
    for k in range(1, 16):
        squares = squares + g_recv[k]
    inverse = to_column(lax.rsqrt(squares / 2048.0 + EPSILON), 64)
    out_ref[...] = (mixed * inverse * ogain[...]).astype(BF16)

    for copy in a1 + a2 + c1 + c2:
        copy.wait_send()

    def drain_kv(d, c):
        lat_copy(d).wait_send()
        g_copy(d, kv, (kv + d) % 16).wait_send()
        return c

    def drain_tp(d, c):
        tp_copy(d, b_send, b_recv, b_ss, b_rs).wait_send()
        tp_copy(d, d_send, d_recv, d_ss, d_rs).wait_send()
        f_copy(d, tp, (tp + d) % 8).wait_send()
        return c

    lax.fori_loop(1, 16, drain_kv, 0)
    lax.fori_loop(1, 8, drain_tp, 0)


def on_device(
    tokens, token_gain, w_query, w_down_kv, w_rope_key, latent_gain, w_key_up, w_value_up, w_out, out_gain,
    cache_latent, cache_rope, lengths,
):
    freq = 1.0 / 10000.0 ** (np.arange(0, 64, 2, dtype=np.float32) / np.float32(64.0))
    freq = jnp.asarray(np.tile(freq.astype(np.float32), 4)[None, :])
    operands = (
        tokens, token_gain.reshape(1, 128), w_query, w_down_kv, w_rope_key, latent_gain.reshape(1, 512),
        w_key_up.reshape(512, 128), w_value_up.reshape(512, 128), w_out, out_gain.reshape(1, 128),
        cache_latent, cache_rope, lengths.reshape(1, 64), freq,
    )
    order = (0, 1, 2, 3, 4, 5, 6, 7, 8, 9, 10, 11, 12, 13)
    local = [pltpu.VMEM(operands[i].shape, operands[i].dtype) for i in order]
    dma = pltpu.SemaphoreType.DMA
    scratch = local + [
        pltpu.VMEM((64, 128), F32), pltpu.VMEM((64, 64), F32), pltpu.VMEM((64, 64), F32),
        pltpu.VMEM((96, 128), BF16), pltpu.VMEM((3, 96, 128), BF16),
        pltpu.VMEM((96, 128), BF16), pltpu.VMEM((3, 96, 128), BF16),
        pltpu.VMEM((64, 640), F32), pltpu.VMEM((8, 1, 640), F32), pltpu.VMEM((16, 1, 640), F32),
        pltpu.VMEM((8, 8, 640), BF16), pltpu.VMEM((8, 8, 640), BF16),
        pltpu.VMEM((8, 8, 640), F32), pltpu.VMEM((64, 640), F32),
        pltpu.VMEM((8, 8, 640), BF16), pltpu.VMEM((8, 8, 640), BF16),
        pltpu.VMEM((64, 128), BF16), pltpu.VMEM((3, 64, 128), BF16),
        pltpu.VMEM((1, 128), F32), pltpu.VMEM((3, 1, 128), F32),
        pltpu.VMEM((64, 128), BF16), pltpu.VMEM((3, 64, 128), BF16),
        pltpu.VMEM((1, 128), F32), pltpu.VMEM((3, 1, 128), F32),
        pltpu.VMEM((8, 64, 128), BF16), pltpu.VMEM((64, 128), BF16),
        pltpu.VMEM((1, 128), F32), pltpu.VMEM((16, 1, 128), F32),
        dma((12,)), dma((16,)),
        dma((3,)), dma((3,)), dma((3,)), dma((3,)), dma((16,)), dma((16,)),
        dma((8,)), dma((8,)), dma((8,)), dma((8,)),
        dma((3,)), dma((3,)), dma((3,)), dma((3,)), dma((3,)), dma((3,)), dma((3,)), dma((3,)),
        dma((8,)), dma((8,)), dma((16,)), dma((16,)),
    ]
    return pl.pallas_call(
        kernel,
        out_shape=jax.ShapeDtypeStruct((64, 128), BF16),
        in_specs=[pl.BlockSpec(memory_space=pl.ANY)] * len(operands),
        out_specs=pl.BlockSpec(memory_space=pltpu.VMEM),
        scratch_shapes=scratch,
        compiler_params=pltpu.CompilerParams(
            collective_id=0, has_side_effects=True, vmem_limit_bytes=48 * 1024 * 1024
        ),
    )(*operands)


def solution(mesh):
    return jax.shard_map(
        on_device,
        mesh=mesh,
        in_specs=(
            P(None, "kv"), P("kv"), P("kv", "tp"), P("kv", None), P("kv", None), P(),
            P("tp", None, None), P("tp", None, None), P("tp", "kv"), P("kv"),
            P("tp", "kv", None), P("tp", "kv", None), P(),
        ),
        out_specs=P(None, "kv"),
        check_vma=False,
    )
```

time: 202 us -> 60.7 us (0.30); the launches traced: 198 us -> 60.2 us
  blocking collectives: 113 us -> 0 us
  Pallas kernels: 0 us -> 46.6 us
  waiting for transfers between devices: 31.6 us -> 0 us
  starting transfers between devices: 18.3 us -> 0 us
  between operations: 13.6 us -> 0.04 us
  matrix products: 11.6 us -> 0 us
  local copies, waits for them, and re-layouts: 2.71 us -> 13.5 us
  other arithmetic: 7.71 us -> 0 us
    all_gather x4 -> x0, blocking collectives: 72.2 us -> none  [over_pieces(): parts = lax.all_gather(value, axis)]
    pallas_call x0 -> x1, Pallas kernels: none -> 46.6 us  [on_device(): pl.pallas_call(kernel, out_shape=jax.ShapeDtypeStruct((64, 128), BF16), i...]
    all_gather x2 -> x0, waiting for transfers between devices: 26.9 us -> none  [over_pieces(): parts = lax.all_gather(value, axis)]
    all_to_all x2 -> x0, starting transfers between devices: 18.2 us -> none  [the longest x1 9.5 us: on_device(): lax.all_to_all(query_rope, 'tp', split_axis=0, concat_axis=1, tiled=True)]
    pmax x2 -> x0, blocking collectives: 14.7 us -> none  [by_axis(): return functools.reduce(lax.pmax, axes, value)]
    psum x2 -> x0, blocking collectives: 14.6 us -> none  [over_axes(): value = lax.psum(value, axis)]
    unnamed x24 -> x26, local copies, waits for them, and re-layouts: 1.87 us -> 13.5 us
    dot_general x10 -> x0, matrix products: 11.6 us -> none  [the longest x1 3.54 us: on_device(): jnp.einsum('bhl,blc->bhc', weights.astype(jnp.bfloat16), cache_latent, pr...]
  transfers between devices with their start and end apart: 4 -> 0, of which waited for: 2 -> 0; matrix products, arithmetic and copies ran while one was open for 6% -> 0% of each run, Pallas kernels for 0% -> 0%
where the time goes in v1:
time: 60.7 us; the launch traced here: 60.2 us
  Pallas kernels  46.6 us (77%)
  local copies, waits for them, and re-layouts  13.5 us (22%)
    pallas_call x1, Pallas kernels, on_device(): pl.pallas_call(kernel, out_shape=jax.ShapeDtypeStruct((64, 128), BF16), i...  46.6 us
    unnamed x26, local copies, waits for them, and re-layouts  13.5 us

profile of v1, /device:TPU:1, one launch (start us, length us, event | category | flops | bytes accessed | tf_op | source)
XLA Modules:
  0.0 60.2 jit_solution(12477124480054222789)
XLA Ops:
  0.0 0.8 %copy.16.wr_h = bf16[128,64]{1,0:T(8,128)(2,1)S(1)} copy(bf16[128,64]{0,1:T(8,128)(2,1)} %param.18) | data formatting | bytes 32768 | tf_op args[4]
  0.8 0.9 %copy.15.wq_h = bf16[128,192]{1,0:T(8,128)(2,1)S(1)} copy(bf16[128,192]{0,1:T(8,128)(2,1)} %param.16) | data formatting | bytes 98304 | tf_op args[2]
  1.7 1.5 %copy.17.cr_h = bf16[8,512,64]{2,1,0:T(8,128)(2,1)S(1)} copy(bf16[8,512,64]{1,2,0:T(8,128)(2,1)} %param.25) | data formatting | bytes 1048576 | tf_op args[11]
  3.3 0.0 copy-start
  3.3 2.2 %copy-done = bf16[8,512,512]{2,1,0:T(8,128)(2,1)S(1)} copy-done((bf16[8,512,512]{2,1,0:T(8,128)(2,1)S(1)}, bf16[8,512,512]{2,1,0:T(8,128)(2,1)}, u32[]{:S(2)}) %copy-start) | copy-done | bytes 4194328
  5.5 0.0 copy-start.1
  5.5 0.9 %copy-done.1 = bf16[128,512]{1,0:T(8,128)(2,1)S(1)} copy-done((bf16[128,512]{1,0:T(8,128)(2,1)S(1)}, bf16[128,512]{1,0:T(8,128)(2,1)}, u32[]{:S(2)}) %copy-start.1) | copy-done | bytes 131096
  6.4 0.0 copy-start.2
  6.4 0.9 %copy-done.2 = bf16[1,512,128]{2,1,0:T(8,128)(2,1)S(1)} copy-done((bf16[1,512,128]{2,1,0:T(8,128)(2,1)S(1)}, bf16[1,512,128]{2,1,0:T(8,128)(2,1)}, u32[]{:S(2)}) %copy-start.2) | copy-done | bytes 131096
  7.3 0.0 copy-start.3
  7.3 0.9 %copy-done.3 = bf16[1,512,128]{2,1,0:T(8,128)(2,1)S(1)} copy-done((bf16[1,512,128]{2,1,0:T(8,128)(2,1)S(1)}, bf16[1,512,128]{2,1,0:T(8,128)(2,1)}, u32[]{:S(2)}) %copy-start.3) | copy-done | bytes 131096
  8.2 0.0 copy-start.4
  8.2 0.8 %copy-done.4 = bf16[128,128]{1,0:T(8,128)(2,1)S(1)} copy-done((bf16[128,128]{1,0:T(8,128)(2,1)S(1)}, bf16[128,128]{1,0:T(8,128)(2,1)}, u32[]{:S(2)}) %copy-start.4) | copy-done | bytes 32792
  8.9 0.0 copy-start.5
  8.9 0.7 %copy-done.5 = bf16[64,128]{1,0:T(8,128)(2,1)S(1)} copy-done((bf16[64,128]{1,0:T(8,128)(2,1)S(1)}, bf16[64,128]{1,0:T(8,128)(2,1)}, u32[]{:S(2)}) %copy-start.5) | copy-done | bytes 16408
  9.6 0.0 copy-start.6
  9.7 0.7 %copy-done.6 = f32[512]{0:T(512)S(1)} copy-done((f32[512]{0:T(512)S(1)}, f32[512]{0:T(512)}, u32[]{:S(2)}) %copy-start.6) | copy-done | bytes 2072
  10.3 0.0 copy-start.7
  10.3 0.7 %copy-done.7 = f32[128]{0:T(128)S(1)} copy-done((f32[128]{0:T(128)S(1)}, f32[128]{0:T(128)}, u32[]{:S(2)}) %copy-start.7) | copy-done | bytes 536
  11.0 0.0 copy-start.8
  11.0 0.7 %copy-done.8 = f32[128]{0:T(128)S(1)} copy-done((f32[128]{0:T(128)S(1)}, f32[128]{0:T(128)}, u32[]{:S(2)}) %copy-start.8) | copy-done | bytes 536
  11.6 0.0 copy-start.9
  11.6 0.7 %copy-done.9 = s32[64]{0:T(128)S(1)} copy-done((s32[64]{0:T(128)S(1)}, s32[64]{0:T(128)}, u32[]{:S(2)}) %copy-start.9) | copy-done | bytes 280
  12.3 0.0 copy-start.10
  12.3 0.7 %copy-done.10 = f32[1,128]{1,0:T(1,128)S(1)} copy-done((f32[1,128]{1,0:T(1,128)S(1)}, f32[1,128]{1,0:T(1,128)}, u32[]{:S(2)}) %copy-start.10) | copy-done | bytes 536
  13.0 46.6 %shard_map.136 = bf16[64,128]{1,0:T(8,128)(2,1)S(1)} custom-call(bf16[64,128]{1,0:T(8,128)(2,1)S(1)} %copy-done.5, f32[1,128]{1,0:T(1,128)S(1)} %bitcast.9, bf16[128,192]{1,0:T(8,128)(2,1)S(1)} %copy.15.wq_h, bf16[128,512]{1,0:T(8,128)(2,1)S(1)} %copy-done.1, bf16[128,64]{1,0:T(8,128)(2,1)S(1)} %copy.16.wr_h, f32[1,512]{1,0:T(1,128)S(1)} %bitcast.8, ...), custom_call_target="tpu_custom_call" | custom-call | tf_op jit(solution)/shard_map/pallas_call | solution.py:410
  59.6 0.6 %copy.19 = bf16[64,128]{1,0:T(8,128)(2,1)} copy(bf16[64,128]{1,0:T(8,128)(2,1)S(1)} %shard_map.136) | data formatting | bytes 32768
Async XLA Ops:
  3.3 2.2 %copy-start = (bf16[8,512,512]{2,1,0:T(8,128)(2,1)S(1)}, bf16[8,512,512]{2,1,0:T(8,128)(2,1)}, u32[]{:S(2)}) copy-start(bf16[8,512,512]{2,1,0:T(8,128)(2,1)} %cl_h.1) | copy-start | bytes 12582916
  5.5 0.9 %copy-start.1 = (bf16[128,512]{1,0:T(8,128)(2,1)S(1)}, bf16[128,512]{1,0:T(8,128)(2,1)}, u32[]{:S(2)}) copy-start(bf16[128,512]{1,0:T(8,128)(2,1)} %wd_h.1) | copy-start | bytes 393220
  6.4 0.9 %copy-start.2 = (bf16[1,512,128]{2,1,0:T(8,128)(2,1)S(1)}, bf16[1,512,128]{2,1,0:T(8,128)(2,1)}, u32[]{:S(2)}) copy-start(bf16[1,512,128]{2,1,0:T(8,128)(2,1)} %param.20) | copy-start | bytes 393220
  7.3 0.9 %copy-start.3 = (bf16[1,512,128]{2,1,0:T(8,128)(2,1)S(1)}, bf16[1,512,128]{2,1,0:T(8,128)(2,1)}, u32[]{:S(2)}) copy-start(bf16[1,512,128]{2,1,0:T(8,128)(2,1)} %param.21) | copy-start | bytes 393220
  8.2 0.8 %copy-start.4 = (bf16[128,128]{1,0:T(8,128)(2,1)S(1)}, bf16[128,128]{1,0:T(8,128)(2,1)}, u32[]{:S(2)}) copy-start(bf16[128,128]{1,0:T(8,128)(2,1)} %wo_h.1) | copy-start | bytes 98308
  8.9 0.7 %copy-start.5 = (bf16[64,128]{1,0:T(8,128)(2,1)S(1)}, bf16[64,128]{1,0:T(8,128)(2,1)}, u32[]{:S(2)}) copy-start(bf16[64,128]{1,0:T(8,128)(2,1)} %tok_h.1) | copy-start | bytes 49156
  9.6 0.7 %copy-start.6 = (f32[512]{0:T(512)S(1)}, f32[512]{0:T(512)}, u32[]{:S(2)}) copy-start(f32[512]{0:T(512)} %param.19) | copy-start | bytes 6148
  10.3 0.7 %copy-start.7 = (f32[128]{0:T(128)S(1)}, f32[128]{0:T(128)}, u32[]{:S(2)}) copy-start(f32[128]{0:T(128)} %param.15) | copy-start | bytes 1540
  11.0 0.7 %copy-start.8 = (f32[128]{0:T(128)S(1)}, f32[128]{0:T(128)}, u32[]{:S(2)}) copy-start(f32[128]{0:T(128)} %param.23) | copy-start | bytes 1540
  11.6 0.7 %copy-start.9 = (s32[64]{0:T(128)S(1)}, s32[64]{0:T(128)}, u32[]{:S(2)}) copy-start(s32[64]{0:T(128)} %param.26) | copy-start | bytes 772
  12.3 0.7 %copy-start.10 = (f32[1,128]{1,0:T(1,128)S(1)}, f32[1,128]{1,0:T(1,128)}, u32[]{:S(2)}) copy-start(f32[1,128]{1,0:T(1,128)} %constant.2.clone.freq_h) | copy-start | bytes 1540

commit v2 on v1

--- a/solution.py
+++ b/solution.py
@@ -86,7 +86,7 @@
     for i in range(3):
         loads[i].wait()
     scaled = (tok[...].astype(F32) * tgain[...]).astype(BF16)
-    q_part = dot(scaled, wq[...])
+    q_part = dot_nt(scaled, wq[...])
     rope_part = q_part[:, 128:192]
     q_nope_part = q_part[:, :128]
     q_rope_part = jnp.concatenate([rope_part[:32], rope_part[32:]], axis=1)
@@ -117,7 +117,7 @@
     for i in range(3, 7):
         loads[i].wait()
     lat_all[:, 0:512] = dot(scaled, wd[...])
-    lat_all[:, 512:576] = dot(scaled, wr[...])
+    lat_all[:, 512:576] = dot_nt(scaled, wr[...])
     lat_all[:, 576:640] = jnp.zeros((64, 64), F32)
     mine = lat_all[pl.ds(pl.multiple_of(tp * 8, 8), 8), :]
     for r in range(8):
@@ -247,7 +247,7 @@
         cache_loads[2 * s].wait()
         cache_loads[2 * s + 1].wait()
         q = q_tab[s].astype(BF16)
-        scores = (dot_nt(q[:, :512], cl[s]) + dot_nt(q[:, 512:576], cr[s])) * factor
+        scores = (dot_nt(q[:, :512], cl[s]) + dot(q[:, 512:576], cr[s])) * factor
         length = len_tab[pl.ds(tp * 8 + s, 1), 0:1]
         visible = positions < length
         is_new = jnp.logical_and(new_seq == s, kv % 2 == 0)
@@ -380,9 +380,9 @@
     freq = 1.0 / 10000.0 ** (np.arange(0, 64, 2, dtype=np.float32) / np.float32(64.0))
     freq = jnp.asarray(np.tile(freq.astype(np.float32), 4)[None, :])
     operands = (
-        tokens, token_gain.reshape(1, 128), w_query, w_down_kv, w_rope_key, latent_gain.reshape(1, 512),
+        tokens, token_gain.reshape(1, 128), w_query.T, w_down_kv, w_rope_key.T, latent_gain.reshape(1, 512),
         w_key_up.reshape(512, 128), w_value_up.reshape(512, 128), w_out, out_gain.reshape(1, 128),
-        cache_latent, cache_rope, lengths.reshape(1, 64), freq,
+        cache_latent, cache_rope.transpose(0, 2, 1), lengths.reshape(1, 64), freq,
     )
     order = (0, 1, 2, 3, 4, 5, 6, 7, 8, 9, 10, 11, 12, 13)
     local = [pltpu.VMEM(operands[i].shape, operands[i].dtype) for i in order]
@@ -414,7 +414,7 @@
         out_specs=pl.BlockSpec(memory_space=pltpu.VMEM),
         scratch_shapes=scratch,
         compiler_params=pltpu.CompilerParams(
-            collective_id=0, has_side_effects=True, vmem_limit_bytes=48 * 1024 * 1024
+            collective_id=0, has_side_effects=True, vmem_limit_bytes=67043328
         ),
     )(*operands)
 

time: 60.7 us -> 47.7 us (0.79)
  local copies, waits for them, and re-layouts: 13.5 us -> 1.32 us
    unnamed x26 -> x1, local copies, waits for them, and re-layouts: 13.5 us -> 1.32 us
where the time goes in v2:
time: 47.7 us; the launch traced here: 47.5 us
  Pallas kernels  46.2 us (97%)
  local copies, waits for them, and re-layouts  1.32 us (3%)
    pallas_call x1, Pallas kernels, on_device(): pl.pallas_call(kernel, out_shape=jax.ShapeDtypeStruct((64, 128), BF16), i...  46.2 us
    unnamed x1, local copies, waits for them, and re-layouts  1.32 us

profile of v2, /device:TPU:1, one launch (start us, length us, event | category | flops | bytes accessed | tf_op | source)
XLA Modules:
  0.0 47.5 jit_solution(3739910255096863447)
XLA Ops:
  0.0 46.2 %shard_map.136 = bf16[64,128]{1,0:T(8,128)(2,1)} custom-call(bf16[64,128]{1,0:T(8,128)(2,1)} %tok_h.1, f32[1,128]{1,0:T(1,128)} %bitcast.15, bf16[192,128]{1,0:T(8,128)(2,1)} %bitcast.12, bf16[128,512]{1,0:T(8,128)(2,1)} %wd_h.1, bf16[64,128]{1,0:T(8,128)(2,1)} %bitcast.13, f32[1,512]{1,0:T(1,128)} %bitcast.14, bf16[512,128]{1,0:T(8,128)(2,1)} %bitcast.10, ...), custom_call_target="tpu_custom_call" | custom-call | tf_op jit(solution)/shard_map/pallas_call | solution.py:410
  46.2 1.3 %copy.16 = bf16[64,128]{1,0:T(8,128)(2,1)} copy(bf16[64,128]{1,0:T(8,128)(2,1)} %shard_map.136) | data formatting | bytes 32768

commit v3 on v2

--- a/solution.py
+++ b/solution.py
@@ -44,12 +44,12 @@
     len_tab, cos_tab, sin_tab,
     a1_send, a1_recv, a2_send, a2_recv,
     lat_all, lat_send, lat_recv,
-    b_send, b_recv, q_tab, o_tab, d_send, d_recv,
+    b_send, b_recv, q_tab, o_tab,
     c1_send, c1_recv, c1_lse, c1_lser, c2_send, c2_recv, c2_lse, c2_lser,
-    f_recv, f_send, g_send, g_recv,
+    m_send, m_recv, g_send, g_recv,
     load_sem, cache_sem,
-    a1_ss, a1_rs, a2_ss, a2_rs, lat_ss, lat_rs, b_ss, b_rs, d_ss, d_rs,
-    c1_ss, c1_rs, c2_ss, c2_rs, cl1_ss, cl1_rs, cl2_ss, cl2_rs, f_ss, f_rs, g_ss, g_rs,
+    a1_ss, a1_rs, a2_ss, a2_rs, lat_ss, lat_rs, b_ss, b_rs, gv_ss, gv_rs, go_ss, go_rs,
+    c1_ss, c1_rs, c2_ss, c2_rs, cl1_ss, cl1_rs, cl2_ss, cl2_rs, m_ss, m_rs, g_ss, g_rs,
 ):
     kv = lax.axis_index("kv")
     tp = lax.axis_index("tp")
@@ -58,20 +58,21 @@
 
     barrier = pltpu.get_barrier_semaphore()
 
-    def greet_kv(d, c):
-        pl.semaphore_signal(barrier, inc=1, device_id=((kv + d) % 16, tp), device_id_type=MESH)
+    def greet_line(d, c):
+        pl.semaphore_signal(barrier, inc=1, device_id=(z * 4 + (x + d) % 4, tp), device_id_type=MESH)
+        pl.semaphore_signal(barrier, inc=1, device_id=((z + d) % 4 * 4 + x, tp), device_id_type=MESH)
         return c
 
     def greet_tp(d, c):
         pl.semaphore_signal(barrier, inc=1, device_id=(kv, (tp + d) % 8), device_id_type=MESH)
         return c
 
-    lax.fori_loop(1, 16, greet_kv, 0)
+    lax.fori_loop(1, 4, greet_line, 0)
     lax.fori_loop(1, 8, greet_tp, 0)
 
     pairs = [
         (tok_h, tok), (tgain_h, tgain), (wq_h, wq), (len_h, lens), (freq_h, freq), (wd_h, wd), (wr_h, wr),
-        (wk_h, wk), (lgain_h, lgain), (wv_h, wv), (wo_h, wo), (ogain_h, ogain),
+        (wk_h, wk), (lgain_h, lgain), (wv_h, wv.at[tp]), (wo_h, wo.at[tp]), (ogain_h, ogain),
     ]
     loads = [pltpu.make_async_copy(s, d, load_sem.at[i]) for i, (s, d) in enumerate(pairs)]
     for copy in loads:
@@ -93,7 +94,7 @@
     a1_send[0:64, :] = q_nope_part.astype(BF16)
     a1_send[64:96, :] = q_rope_part.astype(BF16)
 
-    pl.semaphore_wait(barrier, 22)
+    pl.semaphore_wait(barrier, 13)
 
     def x_dev(d):
         return (z * 4 + (x + d) % 4, tp)
@@ -113,6 +114,31 @@
     a1 = line(a1_send, a1_recv, a1_ss, a1_rs, x_dev)
     for copy in a1:
         copy.start()
+
+    twin = tp + 1 - 2 * (tp % 2)
+
+    def gather_copy(buf, ss, rs, i, slot, to):
+        return pltpu.make_async_remote_copy(
+            src_ref=buf.at[slot], dst_ref=buf.at[slot], send_sem=ss.at[i], recv_sem=rs.at[slot],
+            device_id=(kv, to), device_id_type=MESH,
+        )
+
+    def gather_first(buf, ss, rs):
+        copies = [gather_copy(buf, ss, rs, i, tp, (tp + 2 * d) % 8) for i, d in enumerate((1, 3, 2))]
+        return copies + [gather_copy(buf, ss, rs, 3, tp, twin)]
+
+    def gather_forward(buf, ss, rs):
+        slots = [(tp + 2 * d) % 8 for d in (1, 3, 2)]
+        return [gather_copy(buf, ss, rs, 4 + i, slot, twin) for i, slot in enumerate(slots)]
+
+    loads[9].wait()
+    loads[10].wait()
+    value_sends = gather_first(wv, gv_ss, gv_rs)
+    out_sends = gather_first(wo, go_ss, go_rs)
+    for copy in value_sends + out_sends:
+        copy.start()
+    value_forwards = gather_forward(wv, gv_ss, gv_rs)
+    out_forwards = gather_forward(wo, go_ss, go_rs)
 
     for i in range(3, 7):
         loads[i].wait()
@@ -135,7 +161,6 @@
         lat_copy(d).start()
         return c
 
-    lax.fori_loop(1, 16, lat_start, 0)
 
     len_col = to_column(lens[...].astype(F32), 64)
     len_tab[...] = jnp.broadcast_to(len_col, (64, 128))
@@ -173,6 +198,8 @@
     q_rope = q_rope * cosine + swapped * sine
     q_rope = jnp.concatenate([q_rope[:, :64], q_rope[:, 64:]], axis=0)
 
+    lax.fori_loop(1, 16, lat_start, 0)
+
     loads[7].wait()
     q_lat = dot_nt(q_nope, wk[...])
     pad = jnp.zeros((8, 64), F32)
@@ -202,6 +229,10 @@
             tp_wait_copy(d, src, dst, ss, rs).wait_recv()
 
     tp_exchange(b_send, b_recv, b_ss, b_rs)
+
+    for copy in value_forwards + out_forwards:
+        copy.wait_recv()
+        copy.start()
 
     r64 = iota((64, 64), 0)
     c64 = iota((64, 64), 1)
@@ -268,15 +299,18 @@
             lane8 == 0, hi, jnp.where(lane8 == 1, mid, jnp.where(lane8 == 2, low, 0.0))
         )
 
-    by_head = dot(swap, o_tab[...].astype(BF16))
-    for h in range(8):
-        d_send[h] = by_head[8 * h : 8 * h + 8].astype(BF16)
-    tp_exchange(d_send, d_recv, d_ss, d_rs)
-
-    parts = jnp.concatenate([d_recv[j].astype(F32) for j in range(8)], axis=0)
+    parts = dot(swap, o_tab[...].astype(BF16))
     lse = jnp.sum(parts[:, 512:640], axis=1, keepdims=True)
-    loads[9].wait()
-    value = dot(parts[:, :512].astype(BF16), wv[...])
+
+    def gather_wait(buf, ss, rs):
+        for d in range(4):
+            slot = (twin + 2 * d) % 8
+            gather_copy(buf, ss, rs, 0, slot, twin).wait_recv()
+
+    gather_wait(wv, gv_ss, gv_rs)
+    value = jnp.concatenate(
+        [dot(parts[8 * h : 8 * h + 8, :512].astype(BF16), wv[h]) for h in range(8)], axis=0
+    )
 
     def combine(value, lse, send, recv, lse_send, lse_recv, sems, dev):
         send[...] = value.astype(BF16)
@@ -307,26 +341,23 @@
     value, lse, c2 = combine(
         value, lse, c2_send, c2_recv, c2_lse, c2_lser, (c2_ss, c2_rs, cl2_ss, cl2_rs), z_dev
     )
-    head_out = value.astype(BF16)
-
-    loads[10].wait()
-    f_send[...] = dot(head_out, wo[...]).astype(BF16)
-
-    def f_copy(d, slot, to):
-        return pltpu.make_async_remote_copy(
-            src_ref=f_send, dst_ref=f_recv.at[slot], send_sem=f_ss.at[d], recv_sem=f_rs.at[slot],
+    gather_wait(wo, go_ss, go_rs)
+    head_out = jnp.concatenate([value[8 * h : 8 * h + 8] for h in range(8)], axis=1).astype(BF16)
+    m_send[...] = dot(head_out, wo[...].reshape(1024, 128))
+
+    def m_copy(d, slot, to):
+        return pltpu.make_async_remote_copy(
+            src_ref=m_send, dst_ref=m_recv.at[slot], send_sem=m_ss.at[d], recv_sem=m_rs.at[slot],
             device_id=(kv, to), device_id_type=MESH,
         )
 
     for d in range(1, 8):
-        f_copy(d, tp, (tp + d) % 8).start()
-    f_recv[tp] = f_send[...]
+        m_copy(d, tp, (tp + d) % 8).start()
+    m_recv[tp] = m_send[...]
     for d in range(1, 8):
         frm = (tp + d) % 8
-        f_copy(d, frm, frm).wait_recv()
-    mixed = f_recv[0].astype(F32)
-    for h in range(1, 8):
-        mixed = mixed + f_recv[h].astype(F32)
+        m_copy(d, frm, frm).wait_recv()
+    mixed = m_recv[...].reshape(64, 128)
 
     g_send[...] = to_row(jnp.sum(mixed * mixed, axis=1, keepdims=True), 64)
 
@@ -355,7 +386,7 @@
     inverse = to_column(lax.rsqrt(squares / 2048.0 + EPSILON), 64)
     out_ref[...] = (mixed * inverse * ogain[...]).astype(BF16)
 
-    for copy in a1 + a2 + c1 + c2:
+    for copy in a1 + a2 + c1 + c2 + value_sends + out_sends + value_forwards + out_forwards:
         copy.wait_send()
 
     def drain_kv(d, c):
@@ -365,8 +396,7 @@
 
     def drain_tp(d, c):
         tp_copy(d, b_send, b_recv, b_ss, b_rs).wait_send()
-        tp_copy(d, d_send, d_recv, d_ss, d_rs).wait_send()
-        f_copy(d, tp, (tp + d) % 8).wait_send()
+        m_copy(d, tp, (tp + d) % 8).wait_send()
         return c
 
     lax.fori_loop(1, 16, drain_kv, 0)
@@ -384,8 +414,10 @@
         w_key_up.reshape(512, 128), w_value_up.reshape(512, 128), w_out, out_gain.reshape(1, 128),
         cache_latent, cache_rope.transpose(0, 2, 1), lengths.reshape(1, 64), freq,
     )
-    order = (0, 1, 2, 3, 4, 5, 6, 7, 8, 9, 10, 11, 12, 13)
-    local = [pltpu.VMEM(operands[i].shape, operands[i].dtype) for i in order]
+    shapes = [(a.shape, a.dtype) for a in operands]
+    shapes[7] = ((8, 512, 128), BF16)
+    shapes[8] = ((8, 128, 128), BF16)
+    local = [pltpu.VMEM(*a) for a in shapes]
     dma = pltpu.SemaphoreType.DMA
     scratch = local + [
         pltpu.VMEM((64, 128), F32), pltpu.VMEM((64, 64), F32), pltpu.VMEM((64, 64), F32),
@@ -394,23 +426,22 @@
         pltpu.VMEM((64, 640), F32), pltpu.VMEM((8, 1, 640), F32), pltpu.VMEM((16, 1, 640), F32),
         pltpu.VMEM((8, 8, 640), BF16), pltpu.VMEM((8, 8, 640), BF16),
         pltpu.VMEM((8, 8, 640), F32), pltpu.VMEM((64, 640), F32),
-        pltpu.VMEM((8, 8, 640), BF16), pltpu.VMEM((8, 8, 640), BF16),
         pltpu.VMEM((64, 128), BF16), pltpu.VMEM((3, 64, 128), BF16),
         pltpu.VMEM((1, 128), F32), pltpu.VMEM((3, 1, 128), F32),
         pltpu.VMEM((64, 128), BF16), pltpu.VMEM((3, 64, 128), BF16),
         pltpu.VMEM((1, 128), F32), pltpu.VMEM((3, 1, 128), F32),
-        pltpu.VMEM((8, 64, 128), BF16), pltpu.VMEM((64, 128), BF16),
+        pltpu.VMEM((8, 128), F32), pltpu.VMEM((8, 8, 128), F32),
         pltpu.VMEM((1, 128), F32), pltpu.VMEM((16, 1, 128), F32),
         dma((12,)), dma((16,)),
         dma((3,)), dma((3,)), dma((3,)), dma((3,)), dma((16,)), dma((16,)),
-        dma((8,)), dma((8,)), dma((8,)), dma((8,)),
+        dma((8,)), dma((8,)), dma((8,)), dma((8,)), dma((8,)), dma((8,)),
         dma((3,)), dma((3,)), dma((3,)), dma((3,)), dma((3,)), dma((3,)), dma((3,)), dma((3,)),
         dma((8,)), dma((8,)), dma((16,)), dma((16,)),
     ]
     return pl.pallas_call(
         kernel,
         out_shape=jax.ShapeDtypeStruct((64, 128), BF16),
-        in_specs=[pl.BlockSpec(memory_space=pl.ANY)] * len(operands),
+        in_specs=[pl.BlockSpec(memory_space=pltpu.HBM)] * len(operands),
         out_specs=pl.BlockSpec(memory_space=pltpu.VMEM),
         scratch_shapes=scratch,
         compiler_params=pltpu.CompilerParams(

time: 47.7 us -> 43.8 us (0.918)
  Pallas kernels: 46.2 us -> 42.3 us
    pallas_call x1, Pallas kernels: 46.2 us -> 42.3 us  [on_device(): pl.pallas_call(kernel, out_shape=jax.ShapeDtypeStruct((64, 128), BF16), i...]
where the time goes in v3:
time: 43.8 us; the launch traced here: 43.6 us
  Pallas kernels  42.3 us (97%)
  local copies, waits for them, and re-layouts  1.32 us (3%)
    pallas_call x1, Pallas kernels, on_device(): pl.pallas_call(kernel, out_shape=jax.ShapeDtypeStruct((64, 128), BF16), i...  42.3 us
    unnamed x1, local copies, waits for them, and re-layouts  1.32 us

profile of v3, /device:TPU:1, one launch (start us, length us, event | category | flops | bytes accessed | tf_op | source)
XLA Modules:
  0.0 43.6 jit_solution(6243946103742111114)
XLA Ops:
  0.0 42.3 %shard_map.136 = bf16[64,128]{1,0:T(8,128)(2,1)} custom-call(bf16[64,128]{1,0:T(8,128)(2,1)} %tok_h.1, f32[1,128]{1,0:T(1,128)} %bitcast.15, bf16[192,128]{1,0:T(8,128)(2,1)} %bitcast.12, bf16[128,512]{1,0:T(8,128)(2,1)} %wd_h.1, bf16[64,128]{1,0:T(8,128)(2,1)} %bitcast.13, f32[1,512]{1,0:T(1,128)} %bitcast.14, bf16[512,128]{1,0:T(8,128)(2,1)} %bitcast.10, ...), custom_call_target="tpu_custom_call" | custom-call | tf_op jit(solution)/shard_map/pallas_call | solution.py:441
  42.3 1.3 %copy.16 = bf16[64,128]{1,0:T(8,128)(2,1)} copy(bf16[64,128]{1,0:T(8,128)(2,1)} %shard_map.136) | data formatting | bytes 32768

commit v4 on v3

--- a/solution.py
+++ b/solution.py
@@ -272,32 +272,41 @@
         + jnp.sum(q_new[:, 512:576] * new_rope, axis=1, keepdims=True)
     ) * factor
 
-    positions = (kv * 512 + iota((8, 512), 1)).astype(F32)
-    lane8 = iota((8, 128), 1)
-    for s in range(8):
-        cache_loads[2 * s].wait()
-        cache_loads[2 * s + 1].wait()
-        q = q_tab[s].astype(BF16)
-        scores = (dot_nt(q[:, :512], cl[s]) + dot(q[:, 512:576], cr[s])) * factor
-        length = len_tab[pl.ds(tp * 8 + s, 1), 0:1]
-        visible = positions < length
-        is_new = jnp.logical_and(new_seq == s, kv % 2 == 0)
-        own_new = jnp.where(is_new, new_score, NEGATIVE)
-        top = jnp.maximum(jnp.max(jnp.where(visible, scores, NEGATIVE), axis=1, keepdims=True), own_new)
-        weights = jnp.where(visible, jnp.exp(scores - top), 0.0)
-        new_weight = jnp.where(is_new, jnp.exp(own_new - top), 0.0)
-        total = jnp.sum(weights, axis=1, keepdims=True) + new_weight
-        acc = dot(weights.astype(BF16), cl[s]) + new_weight.astype(BF16).astype(F32) * latent
-        some = total > 0.0
-        safe = jnp.where(some, total, 1.0)
-        lse = jnp.where(some, top + jnp.log(safe), NEGATIVE)
-        hi = lse.astype(BF16).astype(F32)
-        mid = (lse - hi).astype(BF16).astype(F32)
-        low = lse - hi - mid
-        o_tab[8 * s : 8 * s + 8, 0:512] = acc / safe
-        o_tab[8 * s : 8 * s + 8, 512:640] = jnp.where(
-            lane8 == 0, hi, jnp.where(lane8 == 1, mid, jnp.where(lane8 == 2, low, 0.0))
-        )
+    for copy in cache_loads:
+        copy.wait()
+    scores = jnp.concatenate(
+        [
+            dot_nt(q_tab[s].astype(BF16)[:, :512], cl[s]) + dot(q_tab[s].astype(BF16)[:, 512:576], cr[s])
+            for s in range(8)
+        ],
+        axis=0,
+    ) * factor
+    row_seq = iota((64, 1), 0) // 8
+    row_length = jnp.concatenate(
+        [jnp.broadcast_to(len_tab[pl.ds(tp * 8 + s, 1), 0:1], (8, 1)) for s in range(8)], axis=0
+    )
+    positions = (kv * 512 + iota((64, 512), 1)).astype(F32)
+    visible = positions < row_length
+    is_new = jnp.logical_and(row_seq == new_seq, kv % 2 == 0)
+    own_new = jnp.where(is_new, jnp.concatenate([new_score] * 8, axis=0), NEGATIVE)
+    top = jnp.maximum(jnp.max(jnp.where(visible, scores, NEGATIVE), axis=1, keepdims=True), own_new)
+    weights = jnp.where(visible, jnp.exp(scores - top), 0.0)
+    new_weight = jnp.where(is_new, jnp.exp(own_new - top), 0.0)
+    total = jnp.sum(weights, axis=1, keepdims=True) + new_weight
+    some = total > 0.0
+    safe = jnp.where(some, total, 1.0)
+    lse = jnp.where(some, top + jnp.log(safe), NEGATIVE)
+    hi = lse.astype(BF16).astype(F32)
+    mid = (lse - hi).astype(BF16).astype(F32)
+    low = lse - hi - mid
+    lane64 = iota((64, 128), 1)
+    acc = jnp.concatenate(
+        [dot(weights[8 * s : 8 * s + 8].astype(BF16), cl[s]) for s in range(8)], axis=0
+    ) + new_weight.astype(BF16).astype(F32) * latent
+    o_tab[:, 0:512] = acc / safe
+    o_tab[:, 512:640] = jnp.where(
+        lane64 == 0, hi, jnp.where(lane64 == 1, mid, jnp.where(lane64 == 2, low, 0.0))
+    )
 
     parts = dot(swap, o_tab[...].astype(BF16))
     lse = jnp.sum(parts[:, 512:640], axis=1, keepdims=True)

time: 43.8 us -> 41.6 us (0.950)
  Pallas kernels: 42.3 us -> 40.1 us
    pallas_call x1, Pallas kernels: 42.3 us -> 40.1 us  [on_device(): pl.pallas_call(kernel, out_shape=jax.ShapeDtypeStruct((64, 128), BF16), i...]
where the time goes in v4:
time: 41.6 us; the launch traced here: 41.4 us
  Pallas kernels  40.1 us (96%)
  local copies, waits for them, and re-layouts  1.32 us (3%)
    pallas_call x1, Pallas kernels, on_device(): pl.pallas_call(kernel, out_shape=jax.ShapeDtypeStruct((64, 128), BF16), i...  40.1 us
    unnamed x1, local copies, waits for them, and re-layouts  1.32 us

profile of v4, /device:TPU:1, one launch (start us, length us, event | category | flops | bytes accessed | tf_op | source)
XLA Modules:
  0.0 41.4 jit_solution(5136856445546273905)
XLA Ops:
  0.0 40.1 %shard_map.136 = bf16[64,128]{1,0:T(8,128)(2,1)} custom-call(bf16[64,128]{1,0:T(8,128)(2,1)} %tok_h.1, f32[1,128]{1,0:T(1,128)} %bitcast.15, bf16[192,128]{1,0:T(8,128)(2,1)} %bitcast.12, bf16[128,512]{1,0:T(8,128)(2,1)} %wd_h.1, bf16[64,128]{1,0:T(8,128)(2,1)} %bitcast.13, f32[1,512]{1,0:T(1,128)} %bitcast.14, bf16[512,128]{1,0:T(8,128)(2,1)} %bitcast.10, ...), custom_call_target="tpu_custom_call" | custom-call | tf_op jit(solution)/shard_map/pallas_call | solution.py:450
  40.1 1.3 %copy.16 = bf16[64,128]{1,0:T(8,128)(2,1)} copy(bf16[64,128]{1,0:T(8,128)(2,1)} %shard_map.136) | data formatting | bytes 32768

commit v5 on v4

--- a/solution.py
+++ b/solution.py
@@ -48,13 +48,15 @@
     c1_send, c1_recv, c1_lse, c1_lser, c2_send, c2_recv, c2_lse, c2_lser,
     m_send, m_recv, g_send, g_recv,
     load_sem, cache_sem,
-    a1_ss, a1_rs, a2_ss, a2_rs, lat_ss, lat_rs, b_ss, b_rs, gv_ss, gv_rs, go_ss, go_rs,
+    a1_ss, a1_rs, a2_ss, a2_rs, lat_ss, lat_rs, b_ss, b_rs, gv_ss, gv_rs, oy_ss, oy_rs, oz_ss, oz_rs, ot_ss, ot_rs,
     c1_ss, c1_rs, c2_ss, c2_rs, cl1_ss, cl1_rs, cl2_ss, cl2_rs, m_ss, m_rs, g_ss, g_rs,
 ):
     kv = lax.axis_index("kv")
     tp = lax.axis_index("tp")
     z = kv // 4
     x = kv % 4
+    y = tp // 2
+    core = tp % 2
 
     barrier = pltpu.get_barrier_semaphore()
 
@@ -72,7 +74,7 @@
 
     pairs = [
         (tok_h, tok), (tgain_h, tgain), (wq_h, wq), (len_h, lens), (freq_h, freq), (wd_h, wd), (wr_h, wr),
-        (wk_h, wk), (lgain_h, lgain), (wv_h, wv.at[tp]), (wo_h, wo.at[tp]), (ogain_h, ogain),
+        (wk_h, wk), (lgain_h, lgain), (wv_h, wv.at[tp]), (wo_h, wo.at[z, core, y]), (ogain_h, ogain),
     ]
     loads = [pltpu.make_async_copy(s, d, load_sem.at[i]) for i, (s, d) in enumerate(pairs)]
     for copy in loads:
@@ -115,7 +117,7 @@
     for copy in a1:
         copy.start()
 
-    twin = tp + 1 - 2 * (tp % 2)
+    twin = tp + 1 - 2 * core
 
     def gather_copy(buf, ss, rs, i, slot, to):
         return pltpu.make_async_remote_copy(
@@ -134,11 +136,31 @@
     loads[9].wait()
     loads[10].wait()
     value_sends = gather_first(wv, gv_ss, gv_rs)
-    out_sends = gather_first(wo, go_ss, go_rs)
-    for copy in value_sends + out_sends:
+    value_forwards = gather_forward(wv, gv_ss, gv_rs)
+
+    def out_y(d, at):
+        return pltpu.make_async_remote_copy(
+            src_ref=wo.at[z, core, y], dst_ref=wo.at[z, core, at], send_sem=oy_ss.at[d], recv_sem=oy_rs.at[at],
+            device_id=(kv, (tp + 2 * d) % 8), device_id_type=MESH,
+        )
+
+    def out_z(d, at):
+        return pltpu.make_async_remote_copy(
+            src_ref=wo.at[z, core], dst_ref=wo.at[at, core], send_sem=oz_ss.at[d], recv_sem=oz_rs.at[at],
+            device_id=((z + d) % 4 * 4 + x, tp), device_id_type=MESH,
+        )
+
+    def out_twin(d, half):
+        at = (z + d) % 4
+        return pltpu.make_async_remote_copy(
+            src_ref=wo.at[at, core], dst_ref=wo.at[at, half], send_sem=ot_ss.at[d], recv_sem=ot_rs.at[at],
+            device_id=(kv, twin), device_id_type=MESH,
+        )
+
+    for d in (1, 3, 2):
+        out_y(d, y).start()
+    for copy in value_sends:
         copy.start()
-    value_forwards = gather_forward(wv, gv_ss, gv_rs)
-    out_forwards = gather_forward(wo, go_ss, go_rs)
 
     for i in range(3, 7):
         loads[i].wait()
@@ -200,6 +222,12 @@
 
     lax.fori_loop(1, 16, lat_start, 0)
 
+    for d in (1, 3, 2):
+        out_y(d, (y + d) % 4).wait_recv()
+    for d in (1, 3, 2):
+        out_z(d, z).start()
+    out_twin(0, core).start()
+
     loads[7].wait()
     q_lat = dot_nt(q_nope, wk[...])
     pad = jnp.zeros((8, 64), F32)
@@ -230,7 +258,7 @@
 
     tp_exchange(b_send, b_recv, b_ss, b_rs)
 
-    for copy in value_forwards + out_forwards:
+    for copy in value_forwards:
         copy.wait_recv()
         copy.start()
 
@@ -347,12 +375,24 @@
     value, lse, c1 = combine(
         value, lse, c1_send, c1_recv, c1_lse, c1_lser, (c1_ss, c1_rs, cl1_ss, cl1_rs), x_dev
     )
+    for d in (1, 3, 2):
+        out_z(d, (z + d) % 4).wait_recv()
+        out_twin(d, core).start()
+
     value, lse, c2 = combine(
         value, lse, c2_send, c2_recv, c2_lse, c2_lser, (c2_ss, c2_rs, cl2_ss, cl2_rs), z_dev
     )
-    gather_wait(wo, go_ss, go_rs)
-    head_out = jnp.concatenate([value[8 * h : 8 * h + 8] for h in range(8)], axis=1).astype(BF16)
-    m_send[...] = dot(head_out, wo[...].reshape(1024, 128))
+    for d in range(4):
+        out_twin(d, 1 - core).wait_recv()
+    head_out = jnp.concatenate(
+        [value[16 * r + 8 * c : 16 * r + 8 * c + 8] for c in range(2) for r in range(4)], axis=1
+    ).astype(BF16)
+    mixed_z = dot(head_out, jnp.concatenate([wo[k].reshape(1024, 128) for k in range(4)], axis=1))
+    own_mixed = mixed_z[:, 0:128]
+    for k in range(1, 4):
+        own_mixed = jnp.where(z == k, mixed_z[:, 128 * k : 128 * k + 128], own_mixed)
+    m_send[...] = own_mixed
+    g_send[...] = to_row(jnp.sum(mixed_z * mixed_z, axis=1, keepdims=True), 8)
 
     def m_copy(d, slot, to):
         return pltpu.make_async_remote_copy(
@@ -360,47 +400,54 @@
             device_id=(kv, to), device_id_type=MESH,
         )
 
+    place = x * 8 + tp
+
+    def g_copy(d, slot, to):
+        return pltpu.make_async_remote_copy(
+            src_ref=g_send, dst_ref=g_recv.at[slot], send_sem=g_ss.at[d], recv_sem=g_rs.at[slot],
+            device_id=(z * 4 + to // 8, to % 8), device_id_type=MESH,
+        )
+
+    def g_start(d, c):
+        g_copy(d, place, (place + d) % 32).start()
+        return c
+
+    def g_wait(d, c):
+        frm = (place + d) % 32
+        g_copy(d, frm, frm).wait_recv()
+        return c
+
     for d in range(1, 8):
         m_copy(d, tp, (tp + d) % 8).start()
+    lax.fori_loop(1, 32, g_start, 0)
     m_recv[tp] = m_send[...]
+    g_recv[place] = g_send[...]
+    loads[11].wait()
     for d in range(1, 8):
         frm = (tp + d) % 8
         m_copy(d, frm, frm).wait_recv()
+    lax.fori_loop(1, 32, g_wait, 0)
     mixed = m_recv[...].reshape(64, 128)
-
-    g_send[...] = to_row(jnp.sum(mixed * mixed, axis=1, keepdims=True), 64)
-
-    def g_copy(d, slot, to):
-        return pltpu.make_async_remote_copy(
-            src_ref=g_send, dst_ref=g_recv.at[slot], send_sem=g_ss.at[d], recv_sem=g_rs.at[slot],
-            device_id=(to, tp), device_id_type=MESH,
-        )
-
-    def g_start(d, c):
-        g_copy(d, kv, (kv + d) % 16).start()
-        return c
-
-    def g_wait(d, c):
-        frm = (kv + d) % 16
-        g_copy(d, frm, frm).wait_recv()
-        return c
-
-    lax.fori_loop(1, 16, g_start, 0)
-    g_recv[kv] = g_send[...]
-    loads[11].wait()
-    lax.fori_loop(1, 16, g_wait, 0)
-    squares = g_recv[0]
-    for k in range(1, 16):
-        squares = squares + g_recv[k]
-    inverse = to_column(lax.rsqrt(squares / 2048.0 + EPSILON), 64)
+    squares = []
+    for j in range(8):
+        total = g_recv[j]
+        for k in range(1, 4):
+            total = total + g_recv[8 * k + j]
+        squares.append(jnp.broadcast_to(total, (8, 128)))
+    inverse = lax.rsqrt(jnp.concatenate(squares, axis=0) / 2048.0 + EPSILON)
+    picked = iota((64, 128), 0) % 8 == iota((64, 128), 1)
+    inverse = jnp.sum(jnp.where(picked, inverse, 0.0), axis=1, keepdims=True)
     out_ref[...] = (mixed * inverse * ogain[...]).astype(BF16)
 
-    for copy in a1 + a2 + c1 + c2 + value_sends + out_sends + value_forwards + out_forwards:
+    for copy in a1 + a2 + c1 + c2 + value_sends + value_forwards:
         copy.wait_send()
 
     def drain_kv(d, c):
         lat_copy(d).wait_send()
-        g_copy(d, kv, (kv + d) % 16).wait_send()
+        return c
+
+    def drain_plane(d, c):
+        g_copy(d, place, (place + d) % 32).wait_send()
         return c
 
     def drain_tp(d, c):
@@ -408,7 +455,13 @@
         m_copy(d, tp, (tp + d) % 8).wait_send()
         return c
 
+    for d in range(4):
+        out_twin(d, core).wait_send()
+    for d in range(1, 4):
+        out_y(d, y).wait_send()
+        out_z(d, z).wait_send()
     lax.fori_loop(1, 16, drain_kv, 0)
+    lax.fori_loop(1, 32, drain_plane, 0)
     lax.fori_loop(1, 8, drain_tp, 0)
 
 
@@ -425,7 +478,7 @@
     )
     shapes = [(a.shape, a.dtype) for a in operands]
     shapes[7] = ((8, 512, 128), BF16)
-    shapes[8] = ((8, 128, 128), BF16)
+    shapes[8] = ((4, 2, 4, 128, 128), BF16)
     local = [pltpu.VMEM(*a) for a in shapes]
     dma = pltpu.SemaphoreType.DMA
     scratch = local + [
@@ -440,12 +493,13 @@
         pltpu.VMEM((64, 128), BF16), pltpu.VMEM((3, 64, 128), BF16),
         pltpu.VMEM((1, 128), F32), pltpu.VMEM((3, 1, 128), F32),
         pltpu.VMEM((8, 128), F32), pltpu.VMEM((8, 8, 128), F32),
-        pltpu.VMEM((1, 128), F32), pltpu.VMEM((16, 1, 128), F32),
+        pltpu.VMEM((1, 128), F32), pltpu.VMEM((32, 1, 128), F32),
         dma((12,)), dma((16,)),
         dma((3,)), dma((3,)), dma((3,)), dma((3,)), dma((16,)), dma((16,)),
-        dma((8,)), dma((8,)), dma((8,)), dma((8,)), dma((8,)), dma((8,)),
+        dma((8,)), dma((8,)), dma((8,)), dma((8,)),
+        dma((4,)), dma((4,)), dma((4,)), dma((4,)), dma((4,)), dma((4,)),
         dma((3,)), dma((3,)), dma((3,)), dma((3,)), dma((3,)), dma((3,)), dma((3,)), dma((3,)),
-        dma((8,)), dma((8,)), dma((16,)), dma((16,)),
+        dma((8,)), dma((8,)), dma((32,)), dma((32,)),
     ]
     return pl.pallas_call(
         kernel,

time: 41.6 us -> 39.8 us (0.957)
  Pallas kernels: 40.1 us -> 38.3 us
    pallas_call x1, Pallas kernels: 40.1 us -> 38.3 us  [on_device(): pl.pallas_call(kernel, out_shape=jax.ShapeDtypeStruct((64, 128), BF16), i...]
where the time goes in v5:
time: 39.8 us; the launch traced here: 39.6 us
  Pallas kernels  38.3 us (96%)
  local copies, waits for them, and re-layouts  1.32 us (3%)
    pallas_call x1, Pallas kernels, on_device(): pl.pallas_call(kernel, out_shape=jax.ShapeDtypeStruct((64, 128), BF16), i...  38.3 us
    unnamed x1, local copies, waits for them, and re-layouts  1.32 us

profile of v5, /device:TPU:1, one launch (start us, length us, event | category | flops | bytes accessed | tf_op | source)
XLA Modules:
  0.0 39.6 jit_solution(343328381528420368)
XLA Ops:
  0.0 38.3 %shard_map.136 = bf16[64,128]{1,0:T(8,128)(2,1)} custom-call(bf16[64,128]{1,0:T(8,128)(2,1)} %tok_h.1, f32[1,128]{1,0:T(1,128)} %bitcast.15, bf16[192,128]{1,0:T(8,128)(2,1)} %bitcast.12, bf16[128,512]{1,0:T(8,128)(2,1)} %wd_h.1, bf16[64,128]{1,0:T(8,128)(2,1)} %bitcast.13, f32[1,512]{1,0:T(1,128)} %bitcast.14, bf16[512,128]{1,0:T(8,128)(2,1)} %bitcast.10, ...), custom_call_target="tpu_custom_call" | custom-call | tf_op jit(solution)/shard_map/pallas_call | solution.py:504
  38.3 1.3 %copy.16 = bf16[64,128]{1,0:T(8,128)(2,1)} copy(bf16[64,128]{1,0:T(8,128)(2,1)} %shard_map.136) | data formatting | bytes 32768

commit v6 on v5

--- a/solution.py
+++ b/solution.py
@@ -46,8 +46,8 @@
     lat_all, lat_send, lat_recv,
     b_send, b_recv, q_tab, o_tab,
     c1_send, c1_recv, c1_lse, c1_lser, c2_send, c2_recv, c2_lse, c2_lser,
-    m_send, m_recv, g_send, g_recv,
-    load_sem, cache_sem,
+    m_send, m_recv, g_send, g_recv, result,
+    load_sem, cache_sem, result_sem,
     a1_ss, a1_rs, a2_ss, a2_rs, lat_ss, lat_rs, b_ss, b_rs, gv_ss, gv_rs, oy_ss, oy_rs, oz_ss, oz_rs, ot_ss, ot_rs,
     c1_ss, c1_rs, c2_ss, c2_rs, cl1_ss, cl1_rs, cl2_ss, cl2_rs, m_ss, m_rs, g_ss, g_rs,
 ):
@@ -175,7 +175,7 @@
     def lat_copy(d):
         to = (kv + d) % 16
         return pltpu.make_async_remote_copy(
-            src_ref=lat_send.at[to // 2], dst_ref=lat_recv.at[kv], send_sem=lat_ss.at[d], recv_sem=lat_rs.at[kv],
+            src_ref=lat_send.at[to // 2], dst_ref=lat_recv.at[kv], send_sem=lat_ss, recv_sem=lat_rs,
             device_id=(to, tp), device_id_type=MESH,
         )
 
@@ -220,13 +220,6 @@
     q_rope = q_rope * cosine + swapped * sine
     q_rope = jnp.concatenate([q_rope[:, :64], q_rope[:, 64:]], axis=0)
 
-    lax.fori_loop(1, 16, lat_start, 0)
-
-    for d in (1, 3, 2):
-        out_y(d, (y + d) % 4).wait_recv()
-    for d in (1, 3, 2):
-        out_z(d, z).start()
-    out_twin(0, core).start()
 
     loads[7].wait()
     q_lat = dot_nt(q_nope, wk[...])
@@ -235,50 +228,53 @@
         block = jnp.concatenate([q_lat[8 * j : 8 * j + 8], q_rope[8 * j : 8 * j + 8], pad], axis=1)
         b_send[j] = block.astype(BF16)
 
-    def tp_copy(d, src, dst, ss, rs):
+    def b_copy(d):
         to = (tp + d) % 8
         return pltpu.make_async_remote_copy(
-            src_ref=src.at[to], dst_ref=dst.at[tp], send_sem=ss.at[d], recv_sem=rs.at[tp],
+            src_ref=b_send.at[to], dst_ref=b_recv.at[tp], send_sem=b_ss, recv_sem=b_rs,
             device_id=(kv, to), device_id_type=MESH,
         )
 
-    def tp_wait_copy(d, src, dst, ss, rs):
-        frm = (tp + d) % 8
-        return pltpu.make_async_remote_copy(
-            src_ref=src.at[frm], dst_ref=dst.at[frm], send_sem=ss.at[d], recv_sem=rs.at[frm],
-            device_id=(kv, frm), device_id_type=MESH,
-        )
-
-    def tp_exchange(src, dst, ss, rs):
-        for d in range(1, 8):
-            tp_copy(d, src, dst, ss, rs).start()
-        dst[tp] = src[tp]
-        for d in range(1, 8):
-            tp_wait_copy(d, src, dst, ss, rs).wait_recv()
-
-    tp_exchange(b_send, b_recv, b_ss, b_rs)
+    def all_of(ref, count, ss, rs):
+        part = ref.at[pl.ds(0, count)]
+        return pltpu.make_async_remote_copy(
+            src_ref=part, dst_ref=part, send_sem=ss, recv_sem=rs, device_id=(kv, twin), device_id_type=MESH
+        )
+
+    for d in (4, 5, 3, 2, 6, 7, 1):
+        b_copy(d).start()
+    lax.fori_loop(1, 16, lat_start, 0)
+    b_recv[tp] = b_send[tp]
+    for d in (1, 3, 2):
+        out_y(d, (y + d) % 4).wait_recv()
+    for d in (1, 3, 2):
+        out_z(d, z).start()
+    out_twin(0, core).start()
+    all_of(b_recv, 7, b_ss, b_rs).wait_recv()
 
     for copy in value_forwards:
         copy.wait_recv()
         copy.start()
 
-    r64 = iota((64, 64), 0)
-    c64 = iota((64, 64), 1)
-    swap = (c64 == (r64 % 8) * 8 + r64 // 8).astype(BF16)
-    queries = jnp.concatenate([b_recv[h].astype(F32) for h in range(8)], axis=0).astype(BF16)
-    queries = dot(swap, queries)
-    for s in range(8):
-        q_tab[s] = queries[8 * s : 8 * s + 8]
-
-    def lat_wait(d, c):
-        frm = (kv + d) % 16
-        pltpu.make_async_remote_copy(
-            src_ref=lat_send.at[kv // 2], dst_ref=lat_recv.at[frm], send_sem=lat_ss.at[d], recv_sem=lat_rs.at[frm],
-            device_id=(frm, tp), device_id_type=MESH,
-        ).wait_recv()
-        return c
-
-    lax.fori_loop(1, 16, lat_wait, 0)
+    for h in range(8):
+        rows = b_recv[h].astype(F32)
+        for i in range(5):
+            q_tab[i, 8 * h : 8 * h + 8, :] = rows[:, 128 * i : 128 * i + 128]
+
+    def query_of(s):
+        return jnp.concatenate([q_tab[i, pl.ds(s, 8, stride=8), :] for i in range(5)], axis=1)
+
+    for copy in cache_loads:
+        copy.wait()
+    factor = 192.0 ** (-0.5)
+
+    def scores_of(s):
+        q = query_of(s).astype(BF16)
+        return dot_nt(q[:, :512], cl[s]) + dot(q[:, 512:576], cr[s])
+
+    scores = jnp.concatenate([scores_of(s) for s in range(8)], axis=0) * factor
+
+    all_of(lat_recv, 15, lat_ss, lat_rs).wait_recv()
     lat_sum = lat_recv[0]
     for k in range(1, 16):
         lat_sum = lat_sum + lat_recv[k]
@@ -293,22 +289,12 @@
     key_swapped = jnp.concatenate([key_raw[:, 32:], key_raw[:, :32]], axis=1)
     new_rope = key_raw * cos_tab[pl.ds(new_row, 1), :] + key_swapped * sin_tab[pl.ds(new_row, 1), :]
     new_rope = new_rope.astype(BF16).astype(F32)
-    factor = 192.0 ** (-0.5)
-    q_new = q_tab[new_seq]
+    q_new = query_of(new_seq)
     new_score = (
         jnp.sum(q_new[:, :512] * latent, axis=1, keepdims=True)
         + jnp.sum(q_new[:, 512:576] * new_rope, axis=1, keepdims=True)
     ) * factor
 
-    for copy in cache_loads:
-        copy.wait()
-    scores = jnp.concatenate(
-        [
-            dot_nt(q_tab[s].astype(BF16)[:, :512], cl[s]) + dot(q_tab[s].astype(BF16)[:, 512:576], cr[s])
-            for s in range(8)
-        ],
-        axis=0,
-    ) * factor
     row_seq = iota((64, 1), 0) // 8
     row_length = jnp.concatenate(
         [jnp.broadcast_to(len_tab[pl.ds(tp * 8 + s, 1), 0:1], (8, 1)) for s in range(8)], axis=0
@@ -324,20 +310,9 @@
     some = total > 0.0
     safe = jnp.where(some, total, 1.0)
     lse = jnp.where(some, top + jnp.log(safe), NEGATIVE)
-    hi = lse.astype(BF16).astype(F32)
-    mid = (lse - hi).astype(BF16).astype(F32)
-    low = lse - hi - mid
-    lane64 = iota((64, 128), 1)
     acc = jnp.concatenate(
         [dot(weights[8 * s : 8 * s + 8].astype(BF16), cl[s]) for s in range(8)], axis=0
     ) + new_weight.astype(BF16).astype(F32) * latent
-    o_tab[:, 0:512] = acc / safe
-    o_tab[:, 512:640] = jnp.where(
-        lane64 == 0, hi, jnp.where(lane64 == 1, mid, jnp.where(lane64 == 2, low, 0.0))
-    )
-
-    parts = dot(swap, o_tab[...].astype(BF16))
-    lse = jnp.sum(parts[:, 512:640], axis=1, keepdims=True)
 
     def gather_wait(buf, ss, rs):
         for d in range(4):
@@ -345,9 +320,12 @@
             gather_copy(buf, ss, rs, 0, slot, twin).wait_recv()
 
     gather_wait(wv, gv_ss, gv_rs)
-    value = jnp.concatenate(
-        [dot(parts[8 * h : 8 * h + 8, :512].astype(BF16), wv[h]) for h in range(8)], axis=0
-    )
+    by_head = dot(acc.astype(BF16), jnp.concatenate([wv[h] for h in range(8)], axis=1))
+    value = by_head[:, 0:128]
+    row_head = iota((64, 128), 0) % 8
+    for h in range(1, 8):
+        value = jnp.where(row_head == h, by_head[:, 128 * h : 128 * h + 128], value)
+    value = value / safe
 
     def combine(value, lse, send, recv, lse_send, lse_recv, sems, dev):
         send[...] = value.astype(BF16)
@@ -384,8 +362,9 @@
     )
     for d in range(4):
         out_twin(d, 1 - core).wait_recv()
+    o_tab[...] = value
     head_out = jnp.concatenate(
-        [value[16 * r + 8 * c : 16 * r + 8 * c + 8] for c in range(2) for r in range(4)], axis=1
+        [o_tab[pl.ds(2 * r + c, 8, stride=8), :] for c in range(2) for r in range(4)], axis=1
     ).astype(BF16)
     mixed_z = dot(head_out, jnp.concatenate([wo[k].reshape(1024, 128) for k in range(4)], axis=1))
     own_mixed = mixed_z[:, 0:128]
@@ -394,39 +373,43 @@
     m_send[...] = own_mixed
     g_send[...] = to_row(jnp.sum(mixed_z * mixed_z, axis=1, keepdims=True), 8)
 
-    def m_copy(d, slot, to):
-        return pltpu.make_async_remote_copy(
-            src_ref=m_send, dst_ref=m_recv.at[slot], send_sem=m_ss.at[d], recv_sem=m_rs.at[slot],
+    def m_copy(slot, to):
+        return pltpu.make_async_remote_copy(
+            src_ref=m_send, dst_ref=m_recv.at[slot], send_sem=m_ss, recv_sem=m_rs,
             device_id=(kv, to), device_id_type=MESH,
         )
 
     place = x * 8 + tp
 
-    def g_copy(d, slot, to):
-        return pltpu.make_async_remote_copy(
-            src_ref=g_send, dst_ref=g_recv.at[slot], send_sem=g_ss.at[d], recv_sem=g_rs.at[slot],
+    def g_copy(slot, to):
+        return pltpu.make_async_remote_copy(
+            src_ref=g_send, dst_ref=g_recv.at[slot], send_sem=g_ss, recv_sem=g_rs,
             device_id=(z * 4 + to // 8, to % 8), device_id_type=MESH,
         )
 
-    def g_start(d, c):
-        g_copy(d, place, (place + d) % 32).start()
+    def g_start(i, c):
+        g_copy(place, (place + (i + 12) % 31 + 1) % 32).start()
         return c
 
-    def g_wait(d, c):
-        frm = (place + d) % 32
-        g_copy(d, frm, frm).wait_recv()
-        return c
-
-    for d in range(1, 8):
-        m_copy(d, tp, (tp + d) % 8).start()
-    lax.fori_loop(1, 32, g_start, 0)
+    lax.fori_loop(0, 31, g_start, 0)
+    for d in (4, 5, 3, 2, 6, 7, 1):
+        m_copy(tp, (tp + d) % 8).start()
     m_recv[tp] = m_send[...]
     g_recv[place] = g_send[...]
     loads[11].wait()
-    for d in range(1, 8):
-        frm = (tp + d) % 8
-        m_copy(d, frm, frm).wait_recv()
-    lax.fori_loop(1, 32, g_wait, 0)
+
+    for copy in a1 + a2 + c1 + c2 + value_sends + value_forwards:
+        copy.wait_send()
+    for d in range(4):
+        out_twin(d, core).wait_send()
+    for d in range(1, 4):
+        out_y(d, y).wait_send()
+        out_z(d, z).wait_send()
+    all_of(b_recv, 7, b_ss, b_rs).wait_send()
+    all_of(lat_recv, 15, lat_ss, lat_rs).wait_send()
+
+    all_of(m_recv, 7, m_ss, m_rs).wait_recv()
+    all_of(g_recv, 31, g_ss, g_rs).wait_recv()
     mixed = m_recv[...].reshape(64, 128)
     squares = []
     for j in range(8):
@@ -437,32 +420,13 @@
     inverse = lax.rsqrt(jnp.concatenate(squares, axis=0) / 2048.0 + EPSILON)
     picked = iota((64, 128), 0) % 8 == iota((64, 128), 1)
     inverse = jnp.sum(jnp.where(picked, inverse, 0.0), axis=1, keepdims=True)
-    out_ref[...] = (mixed * inverse * ogain[...]).astype(BF16)
-
-    for copy in a1 + a2 + c1 + c2 + value_sends + value_forwards:
-        copy.wait_send()
-
-    def drain_kv(d, c):
-        lat_copy(d).wait_send()
-        return c
-
-    def drain_plane(d, c):
-        g_copy(d, place, (place + d) % 32).wait_send()
-        return c
-
-    def drain_tp(d, c):
-        tp_copy(d, b_send, b_recv, b_ss, b_rs).wait_send()
-        m_copy(d, tp, (tp + d) % 8).wait_send()
-        return c
-
-    for d in range(4):
-        out_twin(d, core).wait_send()
-    for d in range(1, 4):
-        out_y(d, y).wait_send()
-        out_z(d, z).wait_send()
-    lax.fori_loop(1, 16, drain_kv, 0)
-    lax.fori_loop(1, 32, drain_plane, 0)
-    lax.fori_loop(1, 8, drain_tp, 0)
+    result[...] = (mixed * inverse * ogain[...]).astype(BF16)
+    leaving = pltpu.make_async_copy(result, out_ref, result_sem)
+    leaving.start()
+
+    all_of(m_recv, 7, m_ss, m_rs).wait_send()
+    all_of(g_recv, 31, g_ss, g_rs).wait_send()
+    leaving.wait()
 
 
 def on_device(
@@ -487,25 +451,26 @@
         pltpu.VMEM((96, 128), BF16), pltpu.VMEM((3, 96, 128), BF16),
         pltpu.VMEM((64, 640), F32), pltpu.VMEM((8, 1, 640), F32), pltpu.VMEM((16, 1, 640), F32),
         pltpu.VMEM((8, 8, 640), BF16), pltpu.VMEM((8, 8, 640), BF16),
-        pltpu.VMEM((8, 8, 640), F32), pltpu.VMEM((64, 640), F32),
+        pltpu.VMEM((5, 64, 128), F32), pltpu.VMEM((64, 128), F32),
         pltpu.VMEM((64, 128), BF16), pltpu.VMEM((3, 64, 128), BF16),
         pltpu.VMEM((1, 128), F32), pltpu.VMEM((3, 1, 128), F32),
         pltpu.VMEM((64, 128), BF16), pltpu.VMEM((3, 64, 128), BF16),
         pltpu.VMEM((1, 128), F32), pltpu.VMEM((3, 1, 128), F32),
         pltpu.VMEM((8, 128), F32), pltpu.VMEM((8, 8, 128), F32),
         pltpu.VMEM((1, 128), F32), pltpu.VMEM((32, 1, 128), F32),
-        dma((12,)), dma((16,)),
-        dma((3,)), dma((3,)), dma((3,)), dma((3,)), dma((16,)), dma((16,)),
-        dma((8,)), dma((8,)), dma((8,)), dma((8,)),
+        pltpu.VMEM((64, 128), BF16),
+        dma((12,)), dma((16,)), dma,
+        dma((3,)), dma((3,)), dma((3,)), dma((3,)), dma, dma,
+        dma, dma, dma((8,)), dma((8,)),
         dma((4,)), dma((4,)), dma((4,)), dma((4,)), dma((4,)), dma((4,)),
         dma((3,)), dma((3,)), dma((3,)), dma((3,)), dma((3,)), dma((3,)), dma((3,)), dma((3,)),
-        dma((8,)), dma((8,)), dma((32,)), dma((32,)),
+        dma, dma, dma, dma,
     ]
     return pl.pallas_call(
         kernel,
         out_shape=jax.ShapeDtypeStruct((64, 128), BF16),
         in_specs=[pl.BlockSpec(memory_space=pltpu.HBM)] * len(operands),
-        out_specs=pl.BlockSpec(memory_space=pltpu.VMEM),
+        out_specs=pl.BlockSpec(memory_space=pl.ANY),
         scratch_shapes=scratch,
         compiler_params=pltpu.CompilerParams(
             collective_id=0, has_side_effects=True, vmem_limit_bytes=67043328

time: 39.8 us -> 37.9 us (0.952)
  Pallas kernels: 38.3 us -> 36.4 us
    pallas_call x1, Pallas kernels: 38.3 us -> 36.4 us  [on_device(): pl.pallas_call(kernel, out_shape=jax.ShapeDtypeStruct((64, 128), BF16), i...]
where the time goes in v6:
time: 37.9 us; the launch traced here: 37.8 us
  Pallas kernels  36.4 us (96%)
  local copies, waits for them, and re-layouts  1.32 us (3%)
    pallas_call x1, Pallas kernels, on_device(): pl.pallas_call(kernel, out_shape=jax.ShapeDtypeStruct((64, 128), BF16), i...  36.4 us
    unnamed x1, local copies, waits for them, and re-layouts  1.32 us

profile of v6, /device:TPU:1, one launch (start us, length us, event | category | flops | bytes accessed | tf_op | source)
XLA Modules:
  0.0 37.8 jit_solution(4491723274571571422)
XLA Ops:
  0.0 36.4 %shard_map.136 = bf16[64,128]{1,0:T(8,128)(2,1)} custom-call(bf16[64,128]{1,0:T(8,128)(2,1)} %tok_h.1, f32[1,128]{1,0:T(1,128)} %bitcast.15, bf16[192,128]{1,0:T(8,128)(2,1)} %bitcast.12, bf16[128,512]{1,0:T(8,128)(2,1)} %wd_h.1, bf16[64,128]{1,0:T(8,128)(2,1)} %bitcast.13, f32[1,512]{1,0:T(1,128)} %bitcast.14, bf16[512,128]{1,0:T(8,128)(2,1)} %bitcast.10, ...), custom_call_target="tpu_custom_call" | custom-call | tf_op jit(solution)/shard_map/pallas_call | solution.py:469
  36.5 1.3 %copy.16 = bf16[64,128]{1,0:T(8,128)(2,1)} copy(bf16[64,128]{1,0:T(8,128)(2,1)} %shard_map.136) | data formatting | bytes 32768

commit v7 on v6

--- a/solution.py
+++ b/solution.py
@@ -45,11 +45,11 @@
     a1_send, a1_recv, a2_send, a2_recv,
     lat_all, lat_send, lat_recv,
     b_send, b_recv, q_tab, o_tab,
-    c1_send, c1_recv, c1_lse, c1_lser, c2_send, c2_recv, c2_lse, c2_lser,
-    m_send, m_recv, g_send, g_recv, result,
-    load_sem, cache_sem, result_sem,
+    c1_send, c1_recv, c2_send, c2_recv, l_send, l_recv,
+    m_send, m_recv, g_send, g_recv,
+    load_sem, cache_sem,
     a1_ss, a1_rs, a2_ss, a2_rs, lat_ss, lat_rs, b_ss, b_rs, gv_ss, gv_rs, oy_ss, oy_rs, oz_ss, oz_rs, ot_ss, ot_rs,
-    c1_ss, c1_rs, c2_ss, c2_rs, cl1_ss, cl1_rs, cl2_ss, cl2_rs, m_ss, m_rs, g_ss, g_rs,
+    c1_ss, c1_rs, c2_ss, c2_rs, lx_ss, lx_rs, lo_ss, lo_rs, m_ss, m_rs, g_ss, g_rs,
 ):
     kv = lax.axis_index("kv")
     tp = lax.axis_index("tp")
@@ -58,33 +58,31 @@
     y = tp // 2
     core = tp % 2
 
-    barrier = pltpu.get_barrier_semaphore()
-
-    def greet_line(d, c):
-        pl.semaphore_signal(barrier, inc=1, device_id=(z * 4 + (x + d) % 4, tp), device_id_type=MESH)
-        pl.semaphore_signal(barrier, inc=1, device_id=((z + d) % 4 * 4 + x, tp), device_id_type=MESH)
-        return c
-
-    def greet_tp(d, c):
-        pl.semaphore_signal(barrier, inc=1, device_id=(kv, (tp + d) % 8), device_id_type=MESH)
-        return c
-
-    lax.fori_loop(1, 4, greet_line, 0)
-    lax.fori_loop(1, 8, greet_tp, 0)
-
     pairs = [
         (tok_h, tok), (tgain_h, tgain), (wq_h, wq), (len_h, lens), (freq_h, freq), (wd_h, wd), (wr_h, wr),
         (wk_h, wk), (lgain_h, lgain), (wv_h, wv.at[tp]), (wo_h, wo.at[z, core, y]), (ogain_h, ogain),
     ]
     loads = [pltpu.make_async_copy(s, d, load_sem.at[i]) for i, (s, d) in enumerate(pairs)]
-    for copy in loads:
-        copy.start()
     cache_loads = []
     for s in range(8):
         cache_loads.append(pltpu.make_async_copy(cl_h.at[s], cl.at[s], cache_sem.at[s]))
         cache_loads.append(pltpu.make_async_copy(cr_h.at[s], cr.at[s], cache_sem.at[8 + s]))
-    for copy in cache_loads:
-        copy.start()
+    for copy in loads[:3]:
+        copy.start()
+    barrier = pltpu.get_barrier_semaphore()
+
+    def greet_line(d, c):
+        pl.semaphore_signal(barrier, inc=1, device_id=(z * 4 + (x + d) % 4, tp), device_id_type=MESH)
+        pl.semaphore_signal(barrier, inc=1, device_id=((z + d) % 4 * 4 + x, tp), device_id_type=MESH)
+        return c
+
+    def greet_tp(d, c):
+        pl.semaphore_signal(barrier, inc=1, device_id=(kv, (tp + d) % 8), device_id_type=MESH)
+        return c
+
+    lax.fori_loop(1, 4, greet_line, 0)
+    lax.fori_loop(1, 8, greet_tp, 0)
+
 
     for i in range(3):
         loads[i].wait()
@@ -96,6 +94,8 @@
     a1_send[0:64, :] = q_nope_part.astype(BF16)
     a1_send[64:96, :] = q_rope_part.astype(BF16)
 
+    for copy in loads[3:] + cache_loads:
+        copy.start()
     pl.semaphore_wait(barrier, 13)
 
     def x_dev(d):
@@ -327,39 +327,65 @@
         value = jnp.where(row_head == h, by_head[:, 128 * h : 128 * h + 128], value)
     value = value / safe
 
-    def combine(value, lse, send, recv, lse_send, lse_recv, sems, dev):
-        send[...] = value.astype(BF16)
-        lse_send[...] = to_row(lse, 64)
-        copies = line(send, recv, sems[0], sems[1], dev)
-        lse_copies = line(lse_send, lse_recv, sems[2], sems[3], dev)
-        for copy in lse_copies + copies:
-            copy.start()
-        for copy in lse_copies:
-            copy.wait_recv()
-        others = [to_column(lse_recv[d], 64) for d in range(3)]
+    def merge(value, lse, others, recv, copies):
         top = lse
         for other in others:
             top = jnp.maximum(top, other)
         own_scale = jnp.exp(lse - top)
         scales = [jnp.exp(other - top) for other in others]
         total = own_scale + scales[0] + scales[1] + scales[2]
+        merged_scales = [scale / total for scale in scales]
+        merged = value * (own_scale / total)
         for copy in copies:
             copy.wait_recv()
-        merged = value * (own_scale / total)
         for d in range(3):
-            merged = merged + recv[d].astype(F32) * (scales[d] / total)
-        return merged, top + jnp.log(total), copies + lse_copies
-
-    value, lse, c1 = combine(
-        value, lse, c1_send, c1_recv, c1_lse, c1_lser, (c1_ss, c1_rs, cl1_ss, cl1_rs), x_dev
-    )
+            merged = merged + recv[d].astype(F32) * merged_scales[d]
+        return merged, top + jnp.log(total)
+
+    c1_send[...] = value.astype(BF16)
+    l_send[...] = to_row(lse, 64)
+    l_recv[kv] = l_send[...]
+
+    def l_copy(i, ss, rs):
+        to = (z + i // 4) % 4 * 4 + (x + i) % 4
+        return pltpu.make_async_remote_copy(
+            src_ref=l_send, dst_ref=l_recv.at[kv], send_sem=ss, recv_sem=rs,
+            device_id=(to, tp), device_id_type=MESH,
+        )
+
+    def l_start(i, c):
+        l_copy(i, lo_ss, lo_rs).start()
+        return c
+
+    c1 = line(c1_send, c1_recv, c1_ss, c1_rs, x_dev)
+    for i in (2, 1, 3):
+        l_copy(i, lx_ss, lx_rs).start()
+    for copy in (c1[1], c1[0], c1[2]):
+        copy.start()
+    lax.fori_loop(4, 16, l_start, 0)
+    all_of(l_recv, 3, lx_ss, lx_rs).wait_recv()
+    others = [to_column(l_recv[z * 4 + (x + 4 - d) % 4], 64) for d in (1, 2, 3)]
+    value, lse = merge(value, lse, others, c1_recv, c1)
+
     for d in (1, 3, 2):
         out_z(d, (z + d) % 4).wait_recv()
         out_twin(d, core).start()
 
-    value, lse, c2 = combine(
-        value, lse, c2_send, c2_recv, c2_lse, c2_lser, (c2_ss, c2_rs, cl2_ss, cl2_rs), z_dev
-    )
+    c2_send[...] = value.astype(BF16)
+    c2 = line(c2_send, c2_recv, c2_ss, c2_rs, z_dev)
+    for copy in c2:
+        copy.start()
+    all_of(l_recv, 12, lo_ss, lo_rs).wait_recv()
+    others = []
+    for d in (1, 2, 3):
+        rows = [l_recv[(z + 4 - d) % 4 * 4 + i] for i in range(4)]
+        best = jnp.maximum(jnp.maximum(rows[0], rows[1]), jnp.maximum(rows[2], rows[3]))
+        mass = jnp.exp(rows[0] - best)
+        for i in range(1, 4):
+            mass = mass + jnp.exp(rows[i] - best)
+        others.append(to_column(best + jnp.log(mass), 64))
+    value, lse = merge(value, lse, others, c2_recv, c2)
+
     for d in range(4):
         out_twin(d, 1 - core).wait_recv()
     o_tab[...] = value
@@ -407,6 +433,8 @@
         out_z(d, z).wait_send()
     all_of(b_recv, 7, b_ss, b_rs).wait_send()
     all_of(lat_recv, 15, lat_ss, lat_rs).wait_send()
+    all_of(l_recv, 3, lx_ss, lx_rs).wait_send()
+    all_of(l_recv, 12, lo_ss, lo_rs).wait_send()
 
     all_of(m_recv, 7, m_ss, m_rs).wait_recv()
     all_of(g_recv, 31, g_ss, g_rs).wait_recv()
@@ -420,13 +448,10 @@
     inverse = lax.rsqrt(jnp.concatenate(squares, axis=0) / 2048.0 + EPSILON)
     picked = iota((64, 128), 0) % 8 == iota((64, 128), 1)
     inverse = jnp.sum(jnp.where(picked, inverse, 0.0), axis=1, keepdims=True)
-    result[...] = (mixed * inverse * ogain[...]).astype(BF16)
-    leaving = pltpu.make_async_copy(result, out_ref, result_sem)
-    leaving.start()
+    out_ref[...] = (mixed * inverse * ogain[...]).astype(BF16)
 
     all_of(m_recv, 7, m_ss, m_rs).wait_send()
     all_of(g_recv, 31, g_ss, g_rs).wait_send()
-    leaving.wait()
 
 
 def on_device(
@@ -444,6 +469,7 @@
     shapes[7] = ((8, 512, 128), BF16)
     shapes[8] = ((4, 2, 4, 128, 128), BF16)
     local = [pltpu.VMEM(*a) for a in shapes]
+    operands = tuple(pltpu.with_memory_space_constraint(v, pltpu.HBM) for v in operands)
     dma = pltpu.SemaphoreType.DMA
     scratch = local + [
         pltpu.VMEM((64, 128), F32), pltpu.VMEM((64, 64), F32), pltpu.VMEM((64, 64), F32),
@@ -453,27 +479,25 @@
         pltpu.VMEM((8, 8, 640), BF16), pltpu.VMEM((8, 8, 640), BF16),
         pltpu.VMEM((5, 64, 128), F32), pltpu.VMEM((64, 128), F32),
         pltpu.VMEM((64, 128), BF16), pltpu.VMEM((3, 64, 128), BF16),
-        pltpu.VMEM((1, 128), F32), pltpu.VMEM((3, 1, 128), F32),
         pltpu.VMEM((64, 128), BF16), pltpu.VMEM((3, 64, 128), BF16),
-        pltpu.VMEM((1, 128), F32), pltpu.VMEM((3, 1, 128), F32),
+        pltpu.VMEM((1, 128), F32), pltpu.VMEM((16, 1, 128), F32),
         pltpu.VMEM((8, 128), F32), pltpu.VMEM((8, 8, 128), F32),
         pltpu.VMEM((1, 128), F32), pltpu.VMEM((32, 1, 128), F32),
-        pltpu.VMEM((64, 128), BF16),
-        dma((12,)), dma((16,)), dma,
+        dma((12,)), dma((16,)),
         dma((3,)), dma((3,)), dma((3,)), dma((3,)), dma, dma,
         dma, dma, dma((8,)), dma((8,)),
         dma((4,)), dma((4,)), dma((4,)), dma((4,)), dma((4,)), dma((4,)),
-        dma((3,)), dma((3,)), dma((3,)), dma((3,)), dma((3,)), dma((3,)), dma((3,)), dma((3,)),
+        dma((3,)), dma((3,)), dma((3,)), dma((3,)), dma, dma, dma, dma,
         dma, dma, dma, dma,
     ]
     return pl.pallas_call(
         kernel,
-        out_shape=jax.ShapeDtypeStruct((64, 128), BF16),
+        out_shape=pltpu.VMEM((64, 128), BF16),
         in_specs=[pl.BlockSpec(memory_space=pltpu.HBM)] * len(operands),
-        out_specs=pl.BlockSpec(memory_space=pl.ANY),
+        out_specs=pl.BlockSpec(memory_space=pltpu.VMEM),
         scratch_shapes=scratch,
         compiler_params=pltpu.CompilerParams(
-            collective_id=0, has_side_effects=True, vmem_limit_bytes=67043328
+            collective_id=0, has_side_effects=True, vmem_limit_bytes=48 * 1024 * 1024
         ),
     )(*operands)
 

time: 37.9 us -> 36.4 us (0.960)
  Pallas kernels: 36.4 us -> 35.6 us
  local copies, waits for them, and re-layouts: 1.32 us -> 0.61 us
    pallas_call x1, Pallas kernels: 36.4 us -> 35.6 us  [on_device(): pl.pallas_call(kernel, out_shape=pltpu.VMEM((64, 128), BF16), in_specs=[p...]
    unnamed x1, local copies, waits for them, and re-layouts: 1.32 us -> 0.61 us
where the time goes in v7:
time: 36.4 us; the launch traced here: 36.2 us
  Pallas kernels  35.6 us (98%)
  local copies, waits for them, and re-layouts  0.61 us (2%)
    pallas_call x1, Pallas kernels, on_device(): pl.pallas_call(kernel, out_shape=pltpu.VMEM((64, 128), BF16), in_specs=[p...  35.6 us

profile of v7, /device:TPU:1, one launch (start us, length us, event | category | flops | bytes accessed | tf_op | source)
XLA Modules:
  0.0 36.2 jit_solution(10522180256282052529)
XLA Ops:
  0.0 35.6 %shard_map.136 = bf16[64,128]{1,0:T(8,128)(2,1)S(1)} custom-call(bf16[64,128]{1,0:T(8,128)(2,1)} %tok_h.1, f32[1,128]{1,0:T(1,128)} %bitcast.15, bf16[192,128]{1,0:T(8,128)(2,1)} %bitcast.12, bf16[128,512]{1,0:T(8,128)(2,1)} %wd_h.1, bf16[64,128]{1,0:T(8,128)(2,1)} %bitcast.13, f32[1,512]{1,0:T(1,128)} %bitcast.14, bf16[512,128]{1,0:T(8,128)(2,1)} %bitcast.10, ...), custom_call_target="tpu_custom_call" | custom-call | tf_op jit(solution)/shard_map/pallas_call | solution.py:493
  35.6 0.6 %copy.16 = bf16[64,128]{1,0:T(8,128)(2,1)} copy(bf16[64,128]{1,0:T(8,128)(2,1)S(1)} %shard_map.136) | data formatting | bytes 32768

commit v8 on v7

--- a/solution.py
+++ b/solution.py
@@ -172,17 +172,13 @@
         lat_send[r] = mine[r : r + 1, :]
     lat_recv[kv] = lat_send[kv // 2]
 
-    def lat_copy(d):
-        to = (kv + d) % 16
-        return pltpu.make_async_remote_copy(
-            src_ref=lat_send.at[to // 2], dst_ref=lat_recv.at[kv], send_sem=lat_ss, recv_sem=lat_rs,
-            device_id=(to, tp), device_id_type=MESH,
-        )
-
-    def lat_start(d, c):
-        lat_copy(d).start()
-        return c
-
+    def lat_copy(dz, dx):
+        at_z = lax.rem(z + dz, 4)
+        at_x = lax.rem(x + dx, 4)
+        return pltpu.make_async_remote_copy(
+            src_ref=lat_send.at[at_z * 2 + at_x // 2], dst_ref=lat_recv.at[kv], send_sem=lat_ss, recv_sem=lat_rs,
+            device_id=(at_z * 4 + at_x, tp), device_id_type=MESH,
+        )
 
     len_col = to_column(lens[...].astype(F32), 64)
     len_tab[...] = jnp.broadcast_to(len_col, (64, 128))
@@ -212,6 +208,10 @@
     a2 = line(a2_send, a2_recv, a2_ss, a2_rs, z_dev)
     for copy in a2:
         copy.start()
+    for dz in (2, 1, 3, 0):
+        for dx in (2, 1, 3, 0):
+            if (dz, dx) != (0, 0):
+                lat_copy(dz, dx).start()
     for copy in a2:
         copy.wait_recv()
     q_nope = added(q_nope_sum, a2_recv, slice(0, 64)).astype(BF16)
@@ -243,37 +243,12 @@
 
     for d in (4, 5, 3, 2, 6, 7, 1):
         b_copy(d).start()
-    lax.fori_loop(1, 16, lat_start, 0)
     b_recv[tp] = b_send[tp]
     for d in (1, 3, 2):
         out_y(d, (y + d) % 4).wait_recv()
     for d in (1, 3, 2):
         out_z(d, z).start()
     out_twin(0, core).start()
-    all_of(b_recv, 7, b_ss, b_rs).wait_recv()
-
-    for copy in value_forwards:
-        copy.wait_recv()
-        copy.start()
-
-    for h in range(8):
-        rows = b_recv[h].astype(F32)
-        for i in range(5):
-            q_tab[i, 8 * h : 8 * h + 8, :] = rows[:, 128 * i : 128 * i + 128]
-
-    def query_of(s):
-        return jnp.concatenate([q_tab[i, pl.ds(s, 8, stride=8), :] for i in range(5)], axis=1)
-
-    for copy in cache_loads:
-        copy.wait()
-    factor = 192.0 ** (-0.5)
-
-    def scores_of(s):
-        q = query_of(s).astype(BF16)
-        return dot_nt(q[:, :512], cl[s]) + dot(q[:, 512:576], cr[s])
-
-    scores = jnp.concatenate([scores_of(s) for s in range(8)], axis=0) * factor
-
     all_of(lat_recv, 15, lat_ss, lat_rs).wait_recv()
     lat_sum = lat_recv[0]
     for k in range(1, 16):
@@ -289,6 +264,30 @@
     key_swapped = jnp.concatenate([key_raw[:, 32:], key_raw[:, :32]], axis=1)
     new_rope = key_raw * cos_tab[pl.ds(new_row, 1), :] + key_swapped * sin_tab[pl.ds(new_row, 1), :]
     new_rope = new_rope.astype(BF16).astype(F32)
+    all_of(b_recv, 7, b_ss, b_rs).wait_recv()
+
+    for copy in value_forwards:
+        copy.wait_recv()
+        copy.start()
+
+    for h in range(8):
+        rows = b_recv[h].astype(F32)
+        for i in range(5):
+            q_tab[i, 8 * h : 8 * h + 8, :] = rows[:, 128 * i : 128 * i + 128]
+
+    def query_of(s):
+        return jnp.concatenate([q_tab[i, pl.ds(s, 8, stride=8), :] for i in range(5)], axis=1)
+
+    for copy in cache_loads:
+        copy.wait()
+    factor = 192.0 ** (-0.5)
+
+    def scores_of(s):
+        q = query_of(s).astype(BF16)
+        return dot_nt(q[:, :512], cl[s]) + dot(q[:, 512:576], cr[s])
+
+    scores = jnp.concatenate([scores_of(s) for s in range(8)], axis=0) * factor
+
     q_new = query_of(new_seq)
     new_score = (
         jnp.sum(q_new[:, :512] * latent, axis=1, keepdims=True)
@@ -407,17 +406,16 @@
 
     place = x * 8 + tp
 
-    def g_copy(slot, to):
-        return pltpu.make_async_remote_copy(
-            src_ref=g_send, dst_ref=g_recv.at[slot], send_sem=g_ss, recv_sem=g_rs,
-            device_id=(z * 4 + to // 8, to % 8), device_id_type=MESH,
-        )
-
-    def g_start(i, c):
-        g_copy(place, (place + (i + 12) % 31 + 1) % 32).start()
-        return c
-
-    lax.fori_loop(0, 31, g_start, 0)
+    def g_copy(at_x, at_tp):
+        return pltpu.make_async_remote_copy(
+            src_ref=g_send, dst_ref=g_recv.at[place], send_sem=g_ss, recv_sem=g_rs,
+            device_id=(z * 4 + at_x, at_tp), device_id_type=MESH,
+        )
+
+    for dx in (2, 1, 3, 0):
+        for dt in (4, 5, 3, 2, 6, 7, 1, 0):
+            if (dx, dt) != (0, 0):
+                g_copy(lax.rem(x + dx, 4), lax.rem(tp + dt, 8)).start()
     for d in (4, 5, 3, 2, 6, 7, 1):
         m_copy(tp, (tp + d) % 8).start()
     m_recv[tp] = m_send[...]

time: 36.4 us -> 35.1 us (0.964)
  Pallas kernels: 35.6 us -> 34.3 us
    pallas_call x1, Pallas kernels: 35.6 us -> 34.3 us  [on_device(): pl.pallas_call(kernel, out_shape=pltpu.VMEM((64, 128), BF16), in_specs=[p...]
where the time goes in v8:
time: 35.1 us; the launch traced here: 34.9 us
  Pallas kernels  34.3 us (98%)
  local copies, waits for them, and re-layouts  0.61 us (2%)
    pallas_call x1, Pallas kernels, on_device(): pl.pallas_call(kernel, out_shape=pltpu.VMEM((64, 128), BF16), in_specs=[p...  34.3 us

profile of v8, /device:TPU:1, one launch (start us, length us, event | category | flops | bytes accessed | tf_op | source)
XLA Modules:
  0.0 34.9 jit_solution(12019108140494996139)
XLA Ops:
  0.0 34.3 %shard_map.136 = bf16[64,128]{1,0:T(8,128)(2,1)S(1)} custom-call(bf16[64,128]{1,0:T(8,128)(2,1)} %tok_h.1, f32[1,128]{1,0:T(1,128)} %bitcast.15, bf16[192,128]{1,0:T(8,128)(2,1)} %bitcast.12, bf16[128,512]{1,0:T(8,128)(2,1)} %wd_h.1, bf16[64,128]{1,0:T(8,128)(2,1)} %bitcast.13, f32[1,512]{1,0:T(1,128)} %bitcast.14, bf16[512,128]{1,0:T(8,128)(2,1)} %bitcast.10, ...), custom_call_target="tpu_custom_call" | custom-call | tf_op jit(solution)/shard_map/pallas_call | solution.py:491
  34.3 0.6 %copy.16 = bf16[64,128]{1,0:T(8,128)(2,1)} copy(bf16[64,128]{1,0:T(8,128)(2,1)S(1)} %shard_map.136) | data formatting | bytes 32768

commit v9 on v8

--- a/solution.py
+++ b/solution.py
@@ -71,18 +71,15 @@
         copy.start()
     barrier = pltpu.get_barrier_semaphore()
 
-    def greet_line(d, c):
-        pl.semaphore_signal(barrier, inc=1, device_id=(z * 4 + (x + d) % 4, tp), device_id_type=MESH)
-        pl.semaphore_signal(barrier, inc=1, device_id=((z + d) % 4 * 4 + x, tp), device_id_type=MESH)
-        return c
-
-    def greet_tp(d, c):
-        pl.semaphore_signal(barrier, inc=1, device_id=(kv, (tp + d) % 8), device_id_type=MESH)
-        return c
-
-    lax.fori_loop(1, 4, greet_line, 0)
-    lax.fori_loop(1, 8, greet_tp, 0)
-
+    def greet(to_kv, to_tp):
+        pl.semaphore_signal(barrier, inc=1, device_id=(to_kv, to_tp), device_id_type=MESH)
+
+    for d in (2, 1, 3):
+        greet(z * 4 + lax.rem(x + d, 4), tp)
+    for d in (2, 1, 3):
+        greet(lax.rem(z + d, 4) * 4 + x, tp)
+    for d in (4, 5, 3, 2, 6, 7, 1):
+        greet(kv, lax.rem(tp + d, 8))
 
     for i in range(3):
         loads[i].wait()
@@ -104,7 +101,22 @@
     def z_dev(d):
         return (((z + d) % 4) * 4 + x, tp)
 
-    def line(src, dst, ss, rs, dev):
+    def line(src, dst, ss, rs, first, second):
+        half = src.shape[0] // 2
+        copies = []
+        for d in (2, 1, 3):
+            for k, dev in enumerate((first, second)):
+                rows = pl.ds(k * half, half)
+                copies.append(
+                    pltpu.make_async_remote_copy(
+                        src_ref=src.at[rows], dst_ref=dst.at[d - 1, rows],
+                        send_sem=ss.at[3 * k + d - 1], recv_sem=rs.at[3 * k + d - 1],
+                        device_id=dev(d), device_id_type=MESH,
+                    )
+                )
+        return copies
+
+    def line1(src, dst, ss, rs, dev):
         return [
             pltpu.make_async_remote_copy(
                 src_ref=src, dst_ref=dst.at[d - 1], send_sem=ss.at[d - 1], recv_sem=rs.at[d - 1],
@@ -113,7 +125,7 @@
             for d in (1, 2, 3)
         ]
 
-    a1 = line(a1_send, a1_recv, a1_ss, a1_rs, x_dev)
+    a1 = line(a1_send, a1_recv, a1_ss, a1_rs, x_dev, z_dev)
     for copy in a1:
         copy.start()
 
@@ -205,7 +217,7 @@
     q_rope_sum = added(q_rope_part, a1_recv, slice(64, 96))
     a2_send[0:64, :] = q_nope_sum.astype(BF16)
     a2_send[64:96, :] = q_rope_sum.astype(BF16)
-    a2 = line(a2_send, a2_recv, a2_ss, a2_rs, z_dev)
+    a2 = line(a2_send, a2_recv, a2_ss, a2_rs, z_dev, x_dev)
     for copy in a2:
         copy.start()
     for dz in (2, 1, 3, 0):
@@ -309,9 +321,19 @@
     some = total > 0.0
     safe = jnp.where(some, total, 1.0)
     lse = jnp.where(some, top + jnp.log(safe), NEGATIVE)
-    acc = jnp.concatenate(
-        [dot(weights[8 * s : 8 * s + 8].astype(BF16), cl[s]) for s in range(8)], axis=0
-    ) + new_weight.astype(BF16).astype(F32) * latent
+    heads = [dot(weights[8 * s : 8 * s + 8].astype(BF16), cl[s]) for s in range(4)]
+    def l_copy(dz, dx, ss, rs):
+        return pltpu.make_async_remote_copy(
+            src_ref=l_send, dst_ref=l_recv.at[kv], send_sem=ss, recv_sem=rs,
+            device_id=(lax.rem(z + dz, 4) * 4 + lax.rem(x + dx, 4), tp), device_id_type=MESH,
+        )
+
+    l_send[...] = to_row(lse, 64)
+    for d in (2, 1, 3):
+        l_copy(0, d, lx_ss, lx_rs).start()
+    l_recv[kv] = l_send[...]
+    heads += [dot(weights[8 * s : 8 * s + 8].astype(BF16), cl[s]) for s in range(4, 8)]
+    acc = jnp.concatenate(heads, axis=0) + new_weight.astype(BF16).astype(F32) * latent
 
     def gather_wait(buf, ss, rs):
         for d in range(4):
@@ -342,26 +364,12 @@
         return merged, top + jnp.log(total)
 
     c1_send[...] = value.astype(BF16)
-    l_send[...] = to_row(lse, 64)
-    l_recv[kv] = l_send[...]
-
-    def l_copy(i, ss, rs):
-        to = (z + i // 4) % 4 * 4 + (x + i) % 4
-        return pltpu.make_async_remote_copy(
-            src_ref=l_send, dst_ref=l_recv.at[kv], send_sem=ss, recv_sem=rs,
-            device_id=(to, tp), device_id_type=MESH,
-        )
-
-    def l_start(i, c):
-        l_copy(i, lo_ss, lo_rs).start()
-        return c
-
-    c1 = line(c1_send, c1_recv, c1_ss, c1_rs, x_dev)
-    for i in (2, 1, 3):
-        l_copy(i, lx_ss, lx_rs).start()
+    c1 = line1(c1_send, c1_recv, c1_ss, c1_rs, x_dev)
     for copy in (c1[1], c1[0], c1[2]):
         copy.start()
-    lax.fori_loop(4, 16, l_start, 0)
+    for dz in (2, 1, 3):
+        for dx in (2, 1, 3, 0):
+            l_copy(dz, dx, lo_ss, lo_rs).start()
     all_of(l_recv, 3, lx_ss, lx_rs).wait_recv()
     others = [to_column(l_recv[z * 4 + (x + 4 - d) % 4], 64) for d in (1, 2, 3)]
     value, lse = merge(value, lse, others, c1_recv, c1)
@@ -371,7 +379,7 @@
         out_twin(d, core).start()
 
     c2_send[...] = value.astype(BF16)
-    c2 = line(c2_send, c2_recv, c2_ss, c2_rs, z_dev)
+    c2 = line1(c2_send, c2_recv, c2_ss, c2_rs, z_dev)
     for copy in c2:
         copy.start()
     all_of(l_recv, 12, lo_ss, lo_rs).wait_recv()
@@ -482,7 +490,7 @@
         pltpu.VMEM((8, 128), F32), pltpu.VMEM((8, 8, 128), F32),
         pltpu.VMEM((1, 128), F32), pltpu.VMEM((32, 1, 128), F32),
         dma((12,)), dma((16,)),
-        dma((3,)), dma((3,)), dma((3,)), dma((3,)), dma, dma,
+        dma((6,)), dma((6,)), dma((6,)), dma((6,)), dma, dma,
         dma, dma, dma((8,)), dma((8,)),
         dma((4,)), dma((4,)), dma((4,)), dma((4,)), dma((4,)), dma((4,)),
         dma((3,)), dma((3,)), dma((3,)), dma((3,)), dma, dma, dma, dma,

time: 35.1 us -> 34.9 us (level)
  no operation moved by 1% of the time
where the time goes in v9:
time: 34.9 us; the launch traced here: 34.8 us
  Pallas kernels  34.1 us (98%)
  local copies, waits for them, and re-layouts  0.61 us (2%)
    pallas_call x1, Pallas kernels, on_device(): pl.pallas_call(kernel, out_shape=pltpu.VMEM((64, 128), BF16), in_specs=[p...  34.1 us

profile of v9, /device:TPU:1, one launch (start us, length us, event | category | flops | bytes accessed | tf_op | source)
XLA Modules:
  0.0 34.8 jit_solution(7975582528225857984)
XLA Ops:
  0.0 34.1 %shard_map.136 = bf16[64,128]{1,0:T(8,128)(2,1)S(1)} custom-call(bf16[64,128]{1,0:T(8,128)(2,1)} %tok_h.1, f32[1,128]{1,0:T(1,128)} %bitcast.15, bf16[192,128]{1,0:T(8,128)(2,1)} %bitcast.12, bf16[128,512]{1,0:T(8,128)(2,1)} %wd_h.1, bf16[64,128]{1,0:T(8,128)(2,1)} %bitcast.13, f32[1,512]{1,0:T(1,128)} %bitcast.14, bf16[512,128]{1,0:T(8,128)(2,1)} %bitcast.10, ...), custom_call_target="tpu_custom_call" | custom-call | tf_op jit(solution)/shard_map/pallas_call | solution.py:499
  34.2 0.6 %copy.16 = bf16[64,128]{1,0:T(8,128)(2,1)} copy(bf16[64,128]{1,0:T(8,128)(2,1)S(1)} %shard_map.136) | data formatting | bytes 32768

commit v10 on v9

--- a/solution.py
+++ b/solution.py
@@ -44,7 +44,7 @@
     len_tab, cos_tab, sin_tab,
     a1_send, a1_recv, a2_send, a2_recv,
     lat_all, lat_send, lat_recv,
-    b_send, b_recv, q_tab, o_tab,
+    keys, b_send, b_recv, q_tab, o_tab,
     c1_send, c1_recv, c2_send, c2_recv, l_send, l_recv,
     m_send, m_recv, g_send, g_recv,
     load_sem, cache_sem,
@@ -224,6 +224,9 @@
         for dx in (2, 1, 3, 0):
             if (dz, dx) != (0, 0):
                 lat_copy(dz, dx).start()
+    for s in range(4):
+        cache_loads[2 * s].wait()
+        keys[s] = cl[s].T
     for copy in a2:
         copy.wait_recv()
     q_nope = added(q_nope_sum, a2_recv, slice(0, 64)).astype(BF16)
@@ -276,6 +279,9 @@
     key_swapped = jnp.concatenate([key_raw[:, 32:], key_raw[:, :32]], axis=1)
     new_rope = key_raw * cos_tab[pl.ds(new_row, 1), :] + key_swapped * sin_tab[pl.ds(new_row, 1), :]
     new_rope = new_rope.astype(BF16).astype(F32)
+    for s in range(4, 8):
+        cache_loads[2 * s].wait()
+        keys[s] = cl[s].T
     all_of(b_recv, 7, b_ss, b_rs).wait_recv()
 
     for copy in value_forwards:
@@ -290,13 +296,13 @@
     def query_of(s):
         return jnp.concatenate([q_tab[i, pl.ds(s, 8, stride=8), :] for i in range(5)], axis=1)
 
-    for copy in cache_loads:
+    for copy in cache_loads[1::2]:
         copy.wait()
     factor = 192.0 ** (-0.5)
 
     def scores_of(s):
         q = query_of(s).astype(BF16)
-        return dot_nt(q[:, :512], cl[s]) + dot(q[:, 512:576], cr[s])
+        return dot(q[:, :512], keys[s]) + dot(q[:, 512:576], cr[s])
 
     scores = jnp.concatenate([scores_of(s) for s in range(8)], axis=0) * factor
 
@@ -482,6 +488,7 @@
         pltpu.VMEM((96, 128), BF16), pltpu.VMEM((3, 96, 128), BF16),
         pltpu.VMEM((96, 128), BF16), pltpu.VMEM((3, 96, 128), BF16),
         pltpu.VMEM((64, 640), F32), pltpu.VMEM((8, 1, 640), F32), pltpu.VMEM((16, 1, 640), F32),
+        pltpu.VMEM((8, 512, 512), BF16),
         pltpu.VMEM((8, 8, 640), BF16), pltpu.VMEM((8, 8, 640), BF16),
         pltpu.VMEM((5, 64, 128), F32), pltpu.VMEM((64, 128), F32),
         pltpu.VMEM((64, 128), BF16), pltpu.VMEM((3, 64, 128), BF16),

time: 34.9 us -> 34.4 us (0.986)
  Pallas kernels: 34.1 us -> 33.6 us
    pallas_call x1, Pallas kernels: 34.1 us -> 33.6 us  [on_device(): pl.pallas_call(kernel, out_shape=pltpu.VMEM((64, 128), BF16), in_specs=[p...]
where the time goes in v10:
time: 34.4 us; the launch traced here: 34.2 us
  Pallas kernels  33.6 us (98%)
  local copies, waits for them, and re-layouts  0.61 us (2%)
    pallas_call x1, Pallas kernels, on_device(): pl.pallas_call(kernel, out_shape=pltpu.VMEM((64, 128), BF16), in_specs=[p...  33.6 us

profile of v10, /device:TPU:1, one launch (start us, length us, event | category | flops | bytes accessed | tf_op | source)
XLA Modules:
  0.0 34.2 jit_solution(9282827669587582693)
XLA Ops:
  0.0 33.6 %shard_map.136 = bf16[64,128]{1,0:T(8,128)(2,1)S(1)} custom-call(bf16[64,128]{1,0:T(8,128)(2,1)} %tok_h.1, f32[1,128]{1,0:T(1,128)} %bitcast.15, bf16[192,128]{1,0:T(8,128)(2,1)} %bitcast.12, bf16[128,512]{1,0:T(8,128)(2,1)} %wd_h.1, bf16[64,128]{1,0:T(8,128)(2,1)} %bitcast.13, f32[1,512]{1,0:T(1,128)} %bitcast.14, bf16[512,128]{1,0:T(8,128)(2,1)} %bitcast.10, ...), custom_call_target="tpu_custom_call" | custom-call | tf_op jit(solution)/shard_map/pallas_call | solution.py:506
  33.6 0.6 %copy.16 = bf16[64,128]{1,0:T(8,128)(2,1)} copy(bf16[64,128]{1,0:T(8,128)(2,1)S(1)} %shard_map.136) | data formatting | bytes 32768

commit v11 on v10

--- a/solution.py
+++ b/solution.py
@@ -45,11 +45,11 @@
     a1_send, a1_recv, a2_send, a2_recv,
     lat_all, lat_send, lat_recv,
     keys, b_send, b_recv, q_tab, o_tab,
-    c1_send, c1_recv, c2_send, c2_recv, l_send, l_recv,
+    c_send, c_recv, l_send, l_recv,
     m_send, m_recv, g_send, g_recv,
     load_sem, cache_sem,
     a1_ss, a1_rs, a2_ss, a2_rs, lat_ss, lat_rs, b_ss, b_rs, gv_ss, gv_rs, oy_ss, oy_rs, oz_ss, oz_rs, ot_ss, ot_rs,
-    c1_ss, c1_rs, c2_ss, c2_rs, lx_ss, lx_rs, lo_ss, lo_rs, m_ss, m_rs, g_ss, g_rs,
+    c_ss, c_rs, l_ss, l_rs, m_ss, m_rs, g_ss, g_rs,
 ):
     kv = lax.axis_index("kv")
     tp = lax.axis_index("tp")
@@ -236,6 +236,11 @@
     q_rope = jnp.concatenate([q_rope[:, :64], q_rope[:, 64:]], axis=0)
 
 
+    for d in (1, 3, 2):
+        out_y(d, (y + d) % 4).wait_recv()
+    for d in (1, 3, 2):
+        out_z(d, z).start()
+    out_twin(0, core).start()
     loads[7].wait()
     q_lat = dot_nt(q_nope, wk[...])
     pad = jnp.zeros((8, 64), F32)
@@ -259,11 +264,6 @@
     for d in (4, 5, 3, 2, 6, 7, 1):
         b_copy(d).start()
     b_recv[tp] = b_send[tp]
-    for d in (1, 3, 2):
-        out_y(d, (y + d) % 4).wait_recv()
-    for d in (1, 3, 2):
-        out_z(d, z).start()
-    out_twin(0, core).start()
     all_of(lat_recv, 15, lat_ss, lat_rs).wait_recv()
     lat_sum = lat_recv[0]
     for k in range(1, 16):
@@ -328,15 +328,16 @@
     safe = jnp.where(some, total, 1.0)
     lse = jnp.where(some, top + jnp.log(safe), NEGATIVE)
     heads = [dot(weights[8 * s : 8 * s + 8].astype(BF16), cl[s]) for s in range(4)]
-    def l_copy(dz, dx, ss, rs):
-        return pltpu.make_async_remote_copy(
-            src_ref=l_send, dst_ref=l_recv.at[kv], send_sem=ss, recv_sem=rs,
-            device_id=(lax.rem(z + dz, 4) * 4 + lax.rem(x + dx, 4), tp), device_id_type=MESH,
-        )
-
+    def kv_at(dz, dx):
+        return lax.rem(z + dz, 4) * 4 + lax.rem(x + dx, 4)
+
+    others = [(dz, dx) for dz in (2, 1, 3, 0) for dx in (2, 1, 3, 0) if (dz, dx) != (0, 0)]
     l_send[...] = to_row(lse, 64)
-    for d in (2, 1, 3):
-        l_copy(0, d, lx_ss, lx_rs).start()
+    for dz, dx in others:
+        pltpu.make_async_remote_copy(
+            src_ref=l_send, dst_ref=l_recv.at[kv], send_sem=l_ss, recv_sem=l_rs,
+            device_id=(kv_at(dz, dx), tp), device_id_type=MESH,
+        ).start()
     l_recv[kv] = l_send[...]
     heads += [dot(weights[8 * s : 8 * s + 8].astype(BF16), cl[s]) for s in range(4, 8)]
     acc = jnp.concatenate(heads, axis=0) + new_weight.astype(BF16).astype(F32) * latent
@@ -354,89 +355,83 @@
         value = jnp.where(row_head == h, by_head[:, 128 * h : 128 * h + 128], value)
     value = value / safe
 
-    def merge(value, lse, others, recv, copies):
-        top = lse
-        for other in others:
-            top = jnp.maximum(top, other)
-        own_scale = jnp.exp(lse - top)
-        scales = [jnp.exp(other - top) for other in others]
-        total = own_scale + scales[0] + scales[1] + scales[2]
-        merged_scales = [scale / total for scale in scales]
-        merged = value * (own_scale / total)
-        for copy in copies:
-            copy.wait_recv()
-        for d in range(3):
-            merged = merged + recv[d].astype(F32) * merged_scales[d]
-        return merged, top + jnp.log(total)
-
-    c1_send[...] = value.astype(BF16)
-    c1 = line1(c1_send, c1_recv, c1_ss, c1_rs, x_dev)
-    for copy in (c1[1], c1[0], c1[2]):
-        copy.start()
-    for dz in (2, 1, 3):
-        for dx in (2, 1, 3, 0):
-            l_copy(dz, dx, lo_ss, lo_rs).start()
-    all_of(l_recv, 3, lx_ss, lx_rs).wait_recv()
-    others = [to_column(l_recv[z * 4 + (x + 4 - d) % 4], 64) for d in (1, 2, 3)]
-    value, lse = merge(value, lse, others, c1_recv, c1)
+    c_send[...] = value.astype(BF16)
+
+    def c_rows(at_z):
+        return c_send.at[pl.ds(pl.multiple_of(at_z * 16, 16), 16)]
+
+    for dz, dx in others:
+        pltpu.make_async_remote_copy(
+            src_ref=c_rows(lax.rem(z + dz, 4)), dst_ref=c_recv.at[kv], send_sem=c_ss, recv_sem=c_rs,
+            device_id=(kv_at(dz, dx), tp), device_id_type=MESH,
+        ).start()
+    c_recv[kv] = c_send[pl.ds(pl.multiple_of(z * 16, 16), 16), :]
 
     for d in (1, 3, 2):
         out_z(d, (z + d) % 4).wait_recv()
         out_twin(d, core).start()
 
-    c2_send[...] = value.astype(BF16)
-    c2 = line1(c2_send, c2_recv, c2_ss, c2_rs, z_dev)
-    for copy in c2:
-        copy.start()
-    all_of(l_recv, 12, lo_ss, lo_rs).wait_recv()
-    others = []
-    for d in (1, 2, 3):
-        rows = [l_recv[(z + 4 - d) % 4 * 4 + i] for i in range(4)]
-        best = jnp.maximum(jnp.maximum(rows[0], rows[1]), jnp.maximum(rows[2], rows[3]))
-        mass = jnp.exp(rows[0] - best)
-        for i in range(1, 4):
-            mass = mass + jnp.exp(rows[i] - best)
-        others.append(to_column(best + jnp.log(mass), 64))
-    value, lse = merge(value, lse, others, c2_recv, c2)
-
+    all_of(l_recv, 15, l_ss, l_rs).wait_recv()
+    rows = [l_recv[k] for k in range(16)]
+    top_row = functools.reduce(jnp.maximum, rows)
+    masses = [jnp.exp(row - top_row) for row in rows]
+    whole = functools.reduce(jnp.add, masses)
+    own_lane = iota((16, 128), 1) == iota((16, 128), 0) + z * 16
+    shares = [
+        jnp.sum(jnp.where(own_lane, mass / whole, 0.0), axis=1, keepdims=True) for mass in masses
+    ]
+
+    all_of(c_recv, 15, c_ss, c_rs).wait_recv()
+    merged = c_recv[0].astype(F32) * shares[0]
+    for k in range(1, 16):
+        merged = merged + c_recv[k].astype(F32) * shares[k]
+
+    o_tab[...] = merged
     for d in range(4):
         out_twin(d, 1 - core).wait_recv()
-    o_tab[...] = value
     head_out = jnp.concatenate(
-        [o_tab[pl.ds(2 * r + c, 8, stride=8), :] for c in range(2) for r in range(4)], axis=1
+        [o_tab[pl.ds(2 * r + c, 2, stride=8), :] for c in range(2) for r in range(4)], axis=1
     ).astype(BF16)
     mixed_z = dot(head_out, jnp.concatenate([wo[k].reshape(1024, 128) for k in range(4)], axis=1))
-    own_mixed = mixed_z[:, 0:128]
-    for k in range(1, 4):
-        own_mixed = jnp.where(z == k, mixed_z[:, 128 * k : 128 * k + 128], own_mixed)
-    m_send[...] = own_mixed
-    g_send[...] = to_row(jnp.sum(mixed_z * mixed_z, axis=1, keepdims=True), 8)
-
-    def m_copy(slot, to):
-        return pltpu.make_async_remote_copy(
-            src_ref=m_send, dst_ref=m_recv.at[slot], send_sem=m_ss, recv_sem=m_rs,
-            device_id=(kv, to), device_id_type=MESH,
-        )
-
-    place = x * 8 + tp
-
-    def g_copy(at_x, at_tp):
-        return pltpu.make_async_remote_copy(
-            src_ref=g_send, dst_ref=g_recv.at[place], send_sem=g_ss, recv_sem=g_rs,
-            device_id=(z * 4 + at_x, at_tp), device_id_type=MESH,
-        )
-
-    for dx in (2, 1, 3, 0):
+    for k in range(4):
+        m_send[k, :, 0:128] = mixed_z[0:1, 128 * k : 128 * k + 128]
+        m_send[k, :, 128:256] = mixed_z[1:2, 128 * k : 128 * k + 128]
+    g_send[...] = to_row(jnp.sum(mixed_z * mixed_z, axis=1, keepdims=True), 2)
+
+    pair = tp * 4 + z
+
+    def m_start(dz, dt):
+        at_z = lax.rem(z + dz, 4)
+        pltpu.make_async_remote_copy(
+            src_ref=m_send.at[at_z], dst_ref=m_recv.at[pair], send_sem=m_ss, recv_sem=m_rs,
+            device_id=(at_z * 4 + x, lax.rem(tp + dt, 8)), device_id_type=MESH,
+        ).start()
+
+    def g_start(dz, dx, dt):
+        pltpu.make_async_remote_copy(
+            src_ref=g_send, dst_ref=g_recv.at[x * 32 + pair], send_sem=g_ss, recv_sem=g_rs,
+            device_id=(kv_at(dz, dx), lax.rem(tp + dt, 8)), device_id_type=MESH,
+        ).start()
+
+    steps = [(dz, dx, dt) for dz in (2, 1, 3, 0) for dx in (2, 1, 3, 0) for dt in (4, 5, 3, 2, 6, 7, 1, 0)][:-1]
+    hops = [min(dz, 4 - dz) + min(dx, 4 - dx) + min(dt // 2, 4 - dt // 2) for dz, dx, dt in steps]
+    for away in (6, 5, 4):
+        for step, hop in zip(steps, hops):
+            if hop == away:
+                g_start(*step)
+    for dz in (2, 1, 3, 0):
         for dt in (4, 5, 3, 2, 6, 7, 1, 0):
-            if (dx, dt) != (0, 0):
-                g_copy(lax.rem(x + dx, 4), lax.rem(tp + dt, 8)).start()
-    for d in (4, 5, 3, 2, 6, 7, 1):
-        m_copy(tp, (tp + d) % 8).start()
-    m_recv[tp] = m_send[...]
-    g_recv[place] = g_send[...]
+            if (dz, dt) != (0, 0):
+                m_start(dz, dt)
+    for away in (3, 2, 1, 0):
+        for step, hop in zip(steps, hops):
+            if hop == away:
+                g_start(*step)
+    m_recv[pair] = m_send[z]
+    g_recv[x * 32 + pair] = g_send[...]
     loads[11].wait()
 
-    for copy in a1 + a2 + c1 + c2 + value_sends + value_forwards:
+    for copy in a1 + a2 + value_sends + value_forwards:
         copy.wait_send()
     for d in range(4):
         out_twin(d, core).wait_send()
@@ -445,25 +440,35 @@
         out_z(d, z).wait_send()
     all_of(b_recv, 7, b_ss, b_rs).wait_send()
     all_of(lat_recv, 15, lat_ss, lat_rs).wait_send()
-    all_of(l_recv, 3, lx_ss, lx_rs).wait_send()
-    all_of(l_recv, 12, lo_ss, lo_rs).wait_send()
-
-    all_of(m_recv, 7, m_ss, m_rs).wait_recv()
-    all_of(g_recv, 31, g_ss, g_rs).wait_recv()
-    mixed = m_recv[...].reshape(64, 128)
-    squares = []
-    for j in range(8):
-        total = g_recv[j]
-        for k in range(1, 4):
-            total = total + g_recv[8 * k + j]
-        squares.append(jnp.broadcast_to(total, (8, 128)))
-    inverse = lax.rsqrt(jnp.concatenate(squares, axis=0) / 2048.0 + EPSILON)
-    picked = iota((64, 128), 0) % 8 == iota((64, 128), 1)
-    inverse = jnp.sum(jnp.where(picked, inverse, 0.0), axis=1, keepdims=True)
+    all_of(l_recv, 15, l_ss, l_rs).wait_send()
+    all_of(c_recv, 15, c_ss, c_rs).wait_send()
+
+    all_of(m_recv, 31, m_ss, m_rs).wait_recv()
+    all_of(g_recv, 127, g_ss, g_rs).wait_recv()
+    octet = iota((8, 128), 0)
+
+    def eight(of):
+        row = jnp.broadcast_to(of(0), (8, 128))
+        for i in range(1, 8):
+            row = jnp.where(octet == i, of(i), row)
+        return row
+
+    mixed = jnp.concatenate(
+        [
+            eight(lambda i: m_recv[4 * v + i // 2, :, 128 * (i % 2) : 128 * (i % 2) + 128])
+            for v in range(8)
+        ],
+        axis=0,
+    )
+    totals = [g_recv[j] + g_recv[32 + j] + g_recv[64 + j] + g_recv[96 + j] for j in range(32)]
+    squares = jnp.concatenate([eight(lambda i: totals[4 * v + i // 2]) for v in range(8)], axis=0)
+    picked = iota((64, 128), 0) % 2 == iota((64, 128), 1)
+    squares = jnp.sum(jnp.where(picked, squares, 0.0), axis=1, keepdims=True)
+    inverse = lax.rsqrt(squares / 2048.0 + EPSILON)
     out_ref[...] = (mixed * inverse * ogain[...]).astype(BF16)
 
-    all_of(m_recv, 7, m_ss, m_rs).wait_send()
-    all_of(g_recv, 31, g_ss, g_rs).wait_send()
+    all_of(m_recv, 31, m_ss, m_rs).wait_send()
+    all_of(g_recv, 127, g_ss, g_rs).wait_send()
 
 
 def on_device(
@@ -490,18 +495,16 @@
         pltpu.VMEM((64, 640), F32), pltpu.VMEM((8, 1, 640), F32), pltpu.VMEM((16, 1, 640), F32),
         pltpu.VMEM((8, 512, 512), BF16),
         pltpu.VMEM((8, 8, 640), BF16), pltpu.VMEM((8, 8, 640), BF16),
-        pltpu.VMEM((5, 64, 128), F32), pltpu.VMEM((64, 128), F32),
-        pltpu.VMEM((64, 128), BF16), pltpu.VMEM((3, 64, 128), BF16),
-        pltpu.VMEM((64, 128), BF16), pltpu.VMEM((3, 64, 128), BF16),
+        pltpu.VMEM((5, 64, 128), F32), pltpu.VMEM((16, 128), F32),
+        pltpu.VMEM((64, 128), BF16), pltpu.VMEM((16, 16, 128), BF16),
         pltpu.VMEM((1, 128), F32), pltpu.VMEM((16, 1, 128), F32),
-        pltpu.VMEM((8, 128), F32), pltpu.VMEM((8, 8, 128), F32),
-        pltpu.VMEM((1, 128), F32), pltpu.VMEM((32, 1, 128), F32),
+        pltpu.VMEM((4, 1, 256), F32), pltpu.VMEM((32, 1, 256), F32),
+        pltpu.VMEM((1, 128), F32), pltpu.VMEM((128, 1, 128), F32),
         dma((12,)), dma((16,)),
         dma((6,)), dma((6,)), dma((6,)), dma((6,)), dma, dma,
         dma, dma, dma((8,)), dma((8,)),
         dma((4,)), dma((4,)), dma((4,)), dma((4,)), dma((4,)), dma((4,)),
-        dma((3,)), dma((3,)), dma((3,)), dma((3,)), dma, dma, dma, dma,
-        dma, dma, dma, dma,
+        dma, dma, dma, dma, dma, dma, dma, dma,
     ]
     return pl.pallas_call(
         kernel,

time: 34.4 us -> 32.8 us (0.953)
  Pallas kernels: 33.6 us -> 32.1 us
    pallas_call x1, Pallas kernels: 33.6 us -> 32.1 us  [on_device(): pl.pallas_call(kernel, out_shape=pltpu.VMEM((64, 128), BF16), in_specs=[p...]
where the time goes in v11:
time: 32.8 us; the launch traced here: 32.7 us
  Pallas kernels  32.1 us (98%)
  local copies, waits for them, and re-layouts  0.61 us (2%)
    pallas_call x1, Pallas kernels, on_device(): pl.pallas_call(kernel, out_shape=pltpu.VMEM((64, 128), BF16), in_specs=[p...  32.1 us

profile of v11, /device:TPU:1, one launch (start us, length us, event | category | flops | bytes accessed | tf_op | source)
XLA Modules:
  0.0 32.7 jit_solution(4355960592072721238)
XLA Ops:
  0.0 32.1 %shard_map.136 = bf16[64,128]{1,0:T(8,128)(2,1)S(1)} custom-call(bf16[64,128]{1,0:T(8,128)(2,1)} %tok_h.1, f32[1,128]{1,0:T(1,128)} %bitcast.15, bf16[192,128]{1,0:T(8,128)(2,1)} %bitcast.12, bf16[128,512]{1,0:T(8,128)(2,1)} %wd_h.1, bf16[64,128]{1,0:T(8,128)(2,1)} %bitcast.13, f32[1,512]{1,0:T(1,128)} %bitcast.14, bf16[512,128]{1,0:T(8,128)(2,1)} %bitcast.10, ...), custom_call_target="tpu_custom_call" | custom-call | tf_op jit(solution)/shard_map/pallas_call | solution.py:509
  32.1 0.6 %copy.16 = bf16[64,128]{1,0:T(8,128)(2,1)} copy(bf16[64,128]{1,0:T(8,128)(2,1)S(1)} %shard_map.136) | data formatting | bytes 32768

commit v12 on v11

--- a/solution.py
+++ b/solution.py
@@ -44,7 +44,7 @@
     len_tab, cos_tab, sin_tab,
     a1_send, a1_recv, a2_send, a2_recv,
     lat_all, lat_send, lat_recv,
-    keys, b_send, b_recv, q_tab, o_tab,
+    wk_turned, keys, b_send, b_recv, q_tab, o_tab,
     c_send, c_recv, l_send, l_recv,
     m_send, m_recv, g_send, g_recv,
     load_sem, cache_sem,
@@ -67,7 +67,7 @@
     for s in range(8):
         cache_loads.append(pltpu.make_async_copy(cl_h.at[s], cl.at[s], cache_sem.at[s]))
         cache_loads.append(pltpu.make_async_copy(cr_h.at[s], cr.at[s], cache_sem.at[8 + s]))
-    for copy in loads[:3]:
+    for copy in loads[:3] + loads[9:11]:
         copy.start()
     barrier = pltpu.get_barrier_semaphore()
 
@@ -91,7 +91,7 @@
     a1_send[0:64, :] = q_nope_part.astype(BF16)
     a1_send[64:96, :] = q_rope_part.astype(BF16)
 
-    for copy in loads[3:] + cache_loads:
+    for copy in loads[3:9] + loads[11:] + cache_loads:
         copy.start()
     pl.semaphore_wait(barrier, 13)
 
@@ -224,6 +224,8 @@
         for dx in (2, 1, 3, 0):
             if (dz, dx) != (0, 0):
                 lat_copy(dz, dx).start()
+    loads[7].wait()
+    wk_turned[...] = wk[...].T
     for s in range(4):
         cache_loads[2 * s].wait()
         keys[s] = cl[s].T
@@ -241,8 +243,7 @@
     for d in (1, 3, 2):
         out_z(d, z).start()
     out_twin(0, core).start()
-    loads[7].wait()
-    q_lat = dot_nt(q_nope, wk[...])
+    q_lat = dot(q_nope, wk_turned[...])
     pad = jnp.zeros((8, 64), F32)
     for j in range(8):
         block = jnp.concatenate([q_lat[8 * j : 8 * j + 8], q_rope[8 * j : 8 * j + 8], pad], axis=1)
@@ -328,6 +329,9 @@
     safe = jnp.where(some, total, 1.0)
     lse = jnp.where(some, top + jnp.log(safe), NEGATIVE)
     heads = [dot(weights[8 * s : 8 * s + 8].astype(BF16), cl[s]) for s in range(4)]
+    heads += [dot(weights[8 * s : 8 * s + 8].astype(BF16), cl[s]) for s in range(4, 8)]
+    acc = jnp.concatenate(heads, axis=0) + new_weight.astype(BF16).astype(F32) * latent
+
     def kv_at(dz, dx):
         return lax.rem(z + dz, 4) * 4 + lax.rem(x + dx, 4)
 
@@ -339,8 +343,6 @@
             device_id=(kv_at(dz, dx), tp), device_id_type=MESH,
         ).start()
     l_recv[kv] = l_send[...]
-    heads += [dot(weights[8 * s : 8 * s + 8].astype(BF16), cl[s]) for s in range(4, 8)]
-    acc = jnp.concatenate(heads, axis=0) + new_weight.astype(BF16).astype(F32) * latent
 
     def gather_wait(buf, ss, rs):
         for d in range(4):
@@ -382,9 +384,10 @@
     ]
 
     all_of(c_recv, 15, c_ss, c_rs).wait_recv()
-    merged = c_recv[0].astype(F32) * shares[0]
-    for k in range(1, 16):
-        merged = merged + c_recv[k].astype(F32) * shares[k]
+    terms = [c_recv[k].astype(F32) * shares[k] for k in range(16)]
+    while len(terms) > 1:
+        terms = [terms[i] + terms[i + 1] for i in range(0, len(terms), 2)]
+    merged = terms[0]
 
     o_tab[...] = merged
     for d in range(4):
@@ -493,7 +496,7 @@
         pltpu.VMEM((96, 128), BF16), pltpu.VMEM((3, 96, 128), BF16),
         pltpu.VMEM((96, 128), BF16), pltpu.VMEM((3, 96, 128), BF16),
         pltpu.VMEM((64, 640), F32), pltpu.VMEM((8, 1, 640), F32), pltpu.VMEM((16, 1, 640), F32),
-        pltpu.VMEM((8, 512, 512), BF16),
+        pltpu.VMEM((128, 512), BF16), pltpu.VMEM((8, 512, 512), BF16),
         pltpu.VMEM((8, 8, 640), BF16), pltpu.VMEM((8, 8, 640), BF16),
         pltpu.VMEM((5, 64, 128), F32), pltpu.VMEM((16, 128), F32),
         pltpu.VMEM((64, 128), BF16), pltpu.VMEM((16, 16, 128), BF16),

time: 32.8 us -> 32.6 us (level)
  no operation moved by 1% of the time
where the time goes in v12:
time: 32.6 us; the launch traced here: 32.4 us
  Pallas kernels  31.8 us (98%)
  local copies, waits for them, and re-layouts  0.61 us (2%)
    pallas_call x1, Pallas kernels, on_device(): pl.pallas_call(kernel, out_shape=pltpu.VMEM((64, 128), BF16), in_specs=[p...  31.8 us

profile of v12, /device:TPU:1, one launch (start us, length us, event | category | flops | bytes accessed | tf_op | source)
XLA Modules:
  0.0 32.4 jit_solution(12734605436529950736)
XLA Ops:
  0.0 31.8 %shard_map.136 = bf16[64,128]{1,0:T(8,128)(2,1)S(1)} custom-call(bf16[64,128]{1,0:T(8,128)(2,1)} %tok_h.1, f32[1,128]{1,0:T(1,128)} %bitcast.15, bf16[192,128]{1,0:T(8,128)(2,1)} %bitcast.12, bf16[128,512]{1,0:T(8,128)(2,1)} %wd_h.1, bf16[64,128]{1,0:T(8,128)(2,1)} %bitcast.13, f32[1,512]{1,0:T(1,128)} %bitcast.14, bf16[512,128]{1,0:T(8,128)(2,1)} %bitcast.10, ...), custom_call_target="tpu_custom_call" | custom-call | tf_op jit(solution)/shard_map/pallas_call | solution.py:512
  31.8 0.6 %copy.16 = bf16[64,128]{1,0:T(8,128)(2,1)} copy(bf16[64,128]{1,0:T(8,128)(2,1)S(1)} %shard_map.136) | data formatting | bytes 32768

commit v13 on v12

--- a/solution.py
+++ b/solution.py
@@ -138,7 +138,7 @@
         )
 
     def gather_first(buf, ss, rs):
-        copies = [gather_copy(buf, ss, rs, i, tp, (tp + 2 * d) % 8) for i, d in enumerate((1, 3, 2))]
+        copies = [gather_copy(buf, ss, rs, i, tp, (tp + 2 * d) % 8) for i, d in enumerate((2, 1, 3))]
         return copies + [gather_copy(buf, ss, rs, 3, tp, twin)]
 
     def gather_forward(buf, ss, rs):
@@ -169,7 +169,7 @@
             device_id=(kv, twin), device_id_type=MESH,
         )
 
-    for d in (1, 3, 2):
+    for d in (2, 1, 3):
         out_y(d, y).start()
     for copy in value_sends:
         copy.start()
@@ -240,7 +240,7 @@
 
     for d in (1, 3, 2):
         out_y(d, (y + d) % 4).wait_recv()
-    for d in (1, 3, 2):
+    for d in (2, 1, 3):
         out_z(d, z).start()
     out_twin(0, core).start()
     q_lat = dot(q_nope, wk_turned[...])

time: 32.6 us -> 32.6 us (level)
  no operation moved by 1% of the time
where the time goes in v13:
time: 32.6 us; the launch traced here: 32.4 us
  Pallas kernels  31.8 us (98%)
  local copies, waits for them, and re-layouts  0.61 us (2%)
    pallas_call x1, Pallas kernels, on_device(): pl.pallas_call(kernel, out_shape=pltpu.VMEM((64, 128), BF16), in_specs=[p...  31.8 us

profile of v13, /device:TPU:1, one launch (start us, length us, event | category | flops | bytes accessed | tf_op | source)
XLA Modules:
  0.0 32.4 jit_solution(12753120926551726993)
XLA Ops:
  0.0 31.8 %shard_map.136 = bf16[64,128]{1,0:T(8,128)(2,1)S(1)} custom-call(bf16[64,128]{1,0:T(8,128)(2,1)} %tok_h.1, f32[1,128]{1,0:T(1,128)} %bitcast.15, bf16[192,128]{1,0:T(8,128)(2,1)} %bitcast.12, bf16[128,512]{1,0:T(8,128)(2,1)} %wd_h.1, bf16[64,128]{1,0:T(8,128)(2,1)} %bitcast.13, f32[1,512]{1,0:T(1,128)} %bitcast.14, bf16[512,128]{1,0:T(8,128)(2,1)} %bitcast.10, ...), custom_call_target="tpu_custom_call" | custom-call | tf_op jit(solution)/shard_map/pallas_call | solution.py:512
  31.8 0.6 %copy.16 = bf16[64,128]{1,0:T(8,128)(2,1)} copy(bf16[64,128]{1,0:T(8,128)(2,1)S(1)} %shard_map.136) | data formatting | bytes 32768

commit v14 on v13

--- a/solution.py
+++ b/solution.py
@@ -67,8 +67,6 @@
     for s in range(8):
         cache_loads.append(pltpu.make_async_copy(cl_h.at[s], cl.at[s], cache_sem.at[s]))
         cache_loads.append(pltpu.make_async_copy(cr_h.at[s], cr.at[s], cache_sem.at[8 + s]))
-    for copy in loads[:3] + loads[9:11]:
-        copy.start()
     barrier = pltpu.get_barrier_semaphore()
 
     def greet(to_kv, to_tp):
@@ -76,10 +74,11 @@
 
     for d in (2, 1, 3):
         greet(z * 4 + lax.rem(x + d, 4), tp)
-    for d in (2, 1, 3):
         greet(lax.rem(z + d, 4) * 4 + x, tp)
     for d in (4, 5, 3, 2, 6, 7, 1):
         greet(kv, lax.rem(tp + d, 8))
+    for copy in loads[:3] + loads[9:11]:
+        copy.start()
 
     for i in range(3):
         loads[i].wait()

time: 32.6 us -> 32.6 us (level)
  no operation moved by 1% of the time
where the time goes in v14:
time: 32.6 us; the launch traced here: 32.4 us
  Pallas kernels  31.8 us (98%)
  local copies, waits for them, and re-layouts  0.61 us (2%)
    pallas_call x1, Pallas kernels, on_device(): pl.pallas_call(kernel, out_shape=pltpu.VMEM((64, 128), BF16), in_specs=[p...  31.8 us

profile of v14, /device:TPU:1, one launch (start us, length us, event | category | flops | bytes accessed | tf_op | source)
XLA Modules:
  0.0 32.4 jit_solution(18337713260173932888)
XLA Ops:
  0.0 31.8 %shard_map.136 = bf16[64,128]{1,0:T(8,128)(2,1)S(1)} custom-call(bf16[64,128]{1,0:T(8,128)(2,1)} %tok_h.1, f32[1,128]{1,0:T(1,128)} %bitcast.15, bf16[192,128]{1,0:T(8,128)(2,1)} %bitcast.12, bf16[128,512]{1,0:T(8,128)(2,1)} %wd_h.1, bf16[64,128]{1,0:T(8,128)(2,1)} %bitcast.13, f32[1,512]{1,0:T(1,128)} %bitcast.14, bf16[512,128]{1,0:T(8,128)(2,1)} %bitcast.10, ...), custom_call_target="tpu_custom_call" | custom-call | tf_op jit(solution)/shard_map/pallas_call | solution.py:511
  31.8 0.6 %copy.16 = bf16[64,128]{1,0:T(8,128)(2,1)} copy(bf16[64,128]{1,0:T(8,128)(2,1)S(1)} %shard_map.136) | data formatting | bytes 32768

commit v15 on v13

--- a/solution.py
+++ b/solution.py
@@ -45,7 +45,7 @@
     a1_send, a1_recv, a2_send, a2_recv,
     lat_all, lat_send, lat_recv,
     wk_turned, keys, b_send, b_recv, q_tab, o_tab,
-    c_send, c_recv, l_send, l_recv,
+    bias_tab, c_send, c_recv, l_send, l_recv,
     m_send, m_recv, g_send, g_recv,
     load_sem, cache_sem,
     a1_ss, a1_rs, a2_ss, a2_rs, lat_ss, lat_rs, b_ss, b_rs, gv_ss, gv_rs, oy_ss, oy_rs, oz_ss, oz_rs, ot_ss, ot_rs,
@@ -283,6 +283,12 @@
     for s in range(4, 8):
         cache_loads[2 * s].wait()
         keys[s] = cl[s].T
+    row_length = jnp.concatenate(
+        [jnp.broadcast_to(len_tab[pl.ds(tp * 8 + s, 1), 0:1], (8, 1)) for s in range(8)], axis=0
+    )
+    positions = (kv * 512 + iota((64, 512), 1)).astype(F32)
+    visible = positions < row_length
+    bias_tab[...] = jnp.where(visible, 0.0, NEGATIVE)
     all_of(b_recv, 7, b_ss, b_rs).wait_recv()
 
     for copy in value_forwards:
@@ -305,7 +311,7 @@
         q = query_of(s).astype(BF16)
         return dot(q[:, :512], keys[s]) + dot(q[:, 512:576], cr[s])
 
-    scores = jnp.concatenate([scores_of(s) for s in range(8)], axis=0) * factor
+    scores = jnp.concatenate([scores_of(s) for s in range(8)], axis=0) * factor + bias_tab[...]
 
     q_new = query_of(new_seq)
     new_score = (
@@ -314,15 +320,11 @@
     ) * factor
 
     row_seq = iota((64, 1), 0) // 8
-    row_length = jnp.concatenate(
-        [jnp.broadcast_to(len_tab[pl.ds(tp * 8 + s, 1), 0:1], (8, 1)) for s in range(8)], axis=0
-    )
-    positions = (kv * 512 + iota((64, 512), 1)).astype(F32)
-    visible = positions < row_length
     is_new = jnp.logical_and(row_seq == new_seq, kv % 2 == 0)
     own_new = jnp.where(is_new, jnp.concatenate([new_score] * 8, axis=0), NEGATIVE)
-    top = jnp.maximum(jnp.max(jnp.where(visible, scores, NEGATIVE), axis=1, keepdims=True), own_new)
-    weights = jnp.where(visible, jnp.exp(scores - top), 0.0)
+    top = jnp.maximum(jnp.max(scores, axis=1, keepdims=True), own_new)
+    shift = jnp.where(top > 0.5 * NEGATIVE, top, 0.0)
+    weights = jnp.exp(scores - shift)
     new_weight = jnp.where(is_new, jnp.exp(own_new - top), 0.0)
     total = jnp.sum(weights, axis=1, keepdims=True) + new_weight
     some = total > 0.0
@@ -499,7 +501,7 @@
         pltpu.VMEM((128, 512), BF16), pltpu.VMEM((8, 512, 512), BF16),
         pltpu.VMEM((8, 8, 640), BF16), pltpu.VMEM((8, 8, 640), BF16),
         pltpu.VMEM((5, 64, 128), F32), pltpu.VMEM((16, 128), F32),
-        pltpu.VMEM((64, 128), BF16), pltpu.VMEM((16, 16, 128), BF16),
+        pltpu.VMEM((64, 512), F32), pltpu.VMEM((64, 128), BF16), pltpu.VMEM((16, 16, 128), BF16),
         pltpu.VMEM((1, 128), F32), pltpu.VMEM((16, 1, 128), F32),
         pltpu.VMEM((4, 1, 256), F32), pltpu.VMEM((32, 1, 256), F32),
         pltpu.VMEM((1, 128), F32), pltpu.VMEM((128, 1, 128), F32),

time: 32.6 us -> 32.6 us (level)
  no operation moved by 1% of the time
where the time goes in v15:
time: 32.6 us; the launch traced here: 32.4 us
  Pallas kernels  31.8 us (98%)
  local copies, waits for them, and re-layouts  0.61 us (2%)
    pallas_call x1, Pallas kernels, on_device(): pl.pallas_call(kernel, out_shape=pltpu.VMEM((64, 128), BF16), in_specs=[p...  31.8 us

profile of v15, /device:TPU:1, one launch (start us, length us, event | category | flops | bytes accessed | tf_op | source)
XLA Modules:
  0.0 32.4 jit_solution(15952044840480128914)
XLA Ops:
  0.0 31.8 %shard_map.136 = bf16[64,128]{1,0:T(8,128)(2,1)S(1)} custom-call(bf16[64,128]{1,0:T(8,128)(2,1)} %tok_h.1, f32[1,128]{1,0:T(1,128)} %bitcast.15, bf16[192,128]{1,0:T(8,128)(2,1)} %bitcast.12, bf16[128,512]{1,0:T(8,128)(2,1)} %wd_h.1, bf16[64,128]{1,0:T(8,128)(2,1)} %bitcast.13, f32[1,512]{1,0:T(1,128)} %bitcast.14, bf16[512,128]{1,0:T(8,128)(2,1)} %bitcast.10, ...), custom_call_target="tpu_custom_call" | custom-call | tf_op jit(solution)/shard_map/pallas_call | solution.py:514
  31.8 0.6 %copy.16 = bf16[64,128]{1,0:T(8,128)(2,1)} copy(bf16[64,128]{1,0:T(8,128)(2,1)S(1)} %shard_map.136) | data formatting | bytes 32768
